TPU v7x, 128 devices: a whole 4x4x4 slice. The times are simulated.
128 devices in a mesh: st: 64 (over z, y, x), tp: 2 (over core).
Axes of the slice: x: 4, y: 4, z: 4, core: 2. Of those that a mesh axis runs over, the one named last changes fastest.
Arguments:
- tokens: bfloat16 [49152, 2048], P('st'), may hold values from -6 to 6, as said below
- route_ids: int32 [768, 4], P('st'), may hold values from 0 to 1535, as said below
- store: bfloat16 [1536, 128, 2048], P('st'), may hold values from -6 to 6, as said below
- token_gain: float32 [2048], replicated, may hold values from 0.1 to 1.9
- store_gain: float32 [2048], replicated, may hold values from 0.1 to 1.9
- carry_weight: bfloat16 [2048, 512], P(None, 'tp'), may hold values from -0.125 to 0.125
- spatial_weight: bfloat16 [2048, 512], P(None, 'tp'), may hold values from -0.125 to 0.125
- spatial_gain: float32 [512], P('tp'), may hold values from 0.1 to 1.9
- position_mix: bfloat16 [8, 128, 128], P('tp'), may hold values from -0.5 to 0.5
- position_bias: float32 [8, 128], P('tp'), may hold values from 0.1 to 1.9
- query_weight: bfloat16 [2048, 512], P(None, 'tp'), may hold values from -0.86178639 to 0.86178639, as said below
- key_weight: bfloat16 [2048, 512], P(None, 'tp'), may hold values from -0.86178639 to 0.86178639, as said below
- read_weight: bfloat16 [2048, 512], P(None, 'tp'), may hold values from -0.125 to 0.125
- blend_weight: bfloat16 [2048, 512], P(None, 'tp'), may hold values from -0.125 to 0.125
- output_weight: bfloat16 [512, 2048], replicated, may hold values from -0.25 to 0.25
Outputs:
- mixed: bfloat16 [49152, 2048], P(('st', 'tp'))
Inputs may be any that keep to these rules, and one draw needn't show every extreme that they name: `route_ids`: each entry is a passage index; passage p is held by index p // 24 of st. All entries of the spans of one index of st (aligned blocks of 12 rows) are different; they name at most 1 passage held by any one index of st, exactly 1 held by the index before their own (cyclically), and at least one held by the index half the axis away. `tokens`: Activations; in some draws the first token of some spans equals a row of a passage that the span reads. `store`: passage rows. `query_weight`: A projection matrix. `key_weight`: A projection matrix.
All inputs are finite; a program needn't handle non-finite values.
Results may differ from a plain program's by a relative error of at most 0.012.
The roundings to bfloat16 on the way count: a program that leaves them out, or rounds other values in their place, can miss the bound.
Values may be sent and summed in bfloat16 or wider, within the bound.
A program may use at most 128 MiB of HBM per device.

v0:
```python
import jax
import jax.numpy as jnp
from jax import lax
from jax.sharding import PartitionSpec as P

norm_eps = 1e-06


def rms_scaled(matrix, gain_vector):
    values = matrix.astype(jnp.float32)
    scaled = values * lax.rsqrt(jnp.mean(values * values, axis=-1, keepdims=True) + norm_eps)
    return (scaled * gain_vector).astype(jnp.bfloat16)


def passage_partial(queries, key_rows, value_rows):
    score_scale = queries.shape[-1] ** (-0.5)
    scores = (
        jnp.einsum("bthe,bplhe->bpthl", queries, key_rows, preferred_element_type=jnp.float32)
        * score_scale
    )
    score_peak = jnp.max(scores, axis=-1, keepdims=True)
    weights = jnp.exp(scores - score_peak)
    weight_total = jnp.sum(weights, axis=-1)
    summed = jnp.einsum(
        "bpthl,bplhe->bpthe",
        weights.astype(jnp.bfloat16),
        value_rows,
        preferred_element_type=jnp.float32,
    )
    partial_value = (summed / weight_total[..., None]).astype(jnp.bfloat16)
    return (partial_value, score_peak[..., 0] + jnp.log(weight_total))


def merge_partials(partial_value, log_total):
    level_top = jnp.max(log_total, axis=1, keepdims=True)
    weights = jnp.exp(log_total - level_top)
    weight_total = jnp.sum(weights, axis=1)
    summed = jnp.sum(weights[..., None] * partial_value.astype(jnp.float32), axis=1)
    return summed / weight_total[..., None]


def per_device(
    tokens,
    route_ids,
    store,
    token_gain,
    store_gain,
    carry_weight,
    spatial_weight,
    spatial_gain,
    position_mix,
    position_bias,
    query_weight,
    key_weight,
    read_weight,
    blend_weight,
    output_weight,
):
    row_count = tokens.shape[0]
    local_heads = position_mix.shape[0]
    block_length = position_mix.shape[1]
    local_width = carry_weight.shape[1]
    head_dim = local_width // local_heads
    span_count, pick_count = route_ids.shape
    span_length = row_count // span_count
    store_count, passage_length = (store.shape[0], store.shape[1])
    owner_count = lax.axis_size("st")
    requests_total = span_count * pick_count
    capacity = max(1, 2 * requests_total // owner_count)
    flat_ids = route_ids.reshape(requests_total)
    owner_index = flat_ids // store_count
    local_index = flat_ids % store_count
    request_order = jnp.arange(requests_total, dtype=jnp.int32)
    earlier = (owner_index[:, None] == owner_index[None, :]) & (
        request_order[None, :] < request_order[:, None]
    )
    copy_rank = jnp.sum(earlier.astype(jnp.int32), axis=1)
    position = owner_index * capacity + copy_rank
    slot_local = jnp.zeros((owner_count * capacity,), jnp.int32).at[position].set(local_index)
    slot_local = slot_local.reshape(owner_count, capacity)
    store_rows = rms_scaled(store.reshape(store_count * passage_length, store.shape[2]), store_gain)
    store_keys = jnp.dot(store_rows, key_weight, preferred_element_type=jnp.float32).astype(
        jnp.bfloat16
    )
    store_keys = store_keys.reshape(store_count, passage_length, local_heads, head_dim)
    store_values = jnp.dot(store_rows, read_weight, preferred_element_type=jnp.float32).astype(
        jnp.bfloat16
    )
    store_values = store_values.reshape(store_count, passage_length, local_heads, head_dim)
    normed = rms_scaled(tokens, token_gain)
    queries = jnp.dot(normed, query_weight, preferred_element_type=jnp.float32).astype(jnp.bfloat16)
    queries = queries.reshape(span_count, span_length, local_heads, head_dim)
    asked_slots = lax.all_to_all(slot_local, "st", split_axis=0, concat_axis=0, tiled=True)
    sent_keys = store_keys[asked_slots]
    sent_values = store_values[asked_slots]
    got_keys, got_values = (
        lax.all_to_all(sent_keys, "st", split_axis=0, concat_axis=0, tiled=True),
        lax.all_to_all(sent_values, "st", split_axis=0, concat_axis=0, tiled=True),
    )
    slot_shape = (owner_count * capacity, passage_length, local_heads, head_dim)
    span_shape = (span_count, pick_count, passage_length, local_heads, head_dim)
    span_keys = got_keys.reshape(slot_shape)[position].reshape(span_shape)
    span_values = got_values.reshape(slot_shape)[position].reshape(span_shape)
    partial_value, log_total = passage_partial(queries, span_keys, span_values)
    memory = merge_partials(partial_value, log_total).reshape(row_count, local_width)
    carry_branch = jnp.dot(normed, carry_weight, preferred_element_type=jnp.float32)
    spatial = jax.nn.gelu(
        jnp.dot(normed, spatial_weight, preferred_element_type=jnp.float32), approximate=False
    )
    total_width = local_width * lax.axis_size("tp")
    moment_one, moment_two = lax.psum(
        (jnp.sum(spatial, axis=1), jnp.sum(spatial * spatial, axis=1)), "tp"
    )
    channel_mean = (moment_one / total_width)[:, None]
    channel_spread = (moment_two / total_width)[:, None] - channel_mean * channel_mean
    spatial_in = (
        (spatial - channel_mean) * lax.rsqrt(channel_spread + norm_eps) * spatial_gain
    ).astype(jnp.bfloat16)
    blocks = spatial_in.reshape(row_count // block_length, block_length, local_heads, head_dim)
    mixed_blocks = jnp.einsum(
        "hij,njhc->nihc", position_mix, blocks, preferred_element_type=jnp.float32
    )
    mixed_blocks = mixed_blocks + position_bias.T[None, :, :, None]
    gated_mix = jax.nn.gelu(carry_branch, approximate=False) * mixed_blocks.reshape(
        row_count, local_width
    )
    blend_gate = jax.nn.sigmoid(jnp.dot(normed, blend_weight, preferred_element_type=jnp.float32))
    mixed_rows = (gated_mix + blend_gate * memory).astype(jnp.bfloat16)
    by_rows = lax.all_to_all(mixed_rows, "tp", split_axis=0, concat_axis=1, tiled=True)
    return jnp.dot(by_rows, output_weight, preferred_element_type=jnp.float32).astype(jnp.bfloat16)


def solution(mesh):
    in_specs = (
        P("st", None),
        P("st", None),
        P("st", None, None),
        P(),
        P(),
        P(None, "tp"),
        P(None, "tp"),
        P("tp"),
        P("tp", None, None),
        P("tp", None),
        P(None, "tp"),
        P(None, "tp"),
        P(None, "tp"),
        P(None, "tp"),
        P(),
    )
    out_specs = P(("st", "tp"), None)
    return jax.shard_map(
        per_device, mesh=mesh, in_specs=in_specs, out_specs=out_specs, check_vma=False
    )
```

profile of v0, /device:TPU:1, one launch (start us, length us, event | category | flops | bytes accessed | tf_op | source)
XLA Modules:
  0.0 213.6 jit_solution(6045891707211936595)
XLA Ops:
  0.0 0.8 compare_and_fusion
  0.8 0.7 broadcast_remainder_fusion
  2.4 0.2 convert_reduce_fusion
  2.6 0.7 scatter_custom_fusion
  3.4 0.7 copy.134
  4.0 12.0 %all-to-all-start = ((s32[64,1,1]{2,1,0:T(1,128)}), s32[64,1,1]{2,1,0:T(1,128)S(1)}, u32[]{:S(2)}, u32[]{:S(2)}) async-start(s32[64,1,1]{2,1,0:T(1,128)} %copy.134), calls=%async_computation | async-start | bytes 65536 | tf_op jit(solution)/shard_map/all_to_all | solution.py:93
  16.0 7.1 %multiply_reduce_fusion = f32[24,128]{1,0:T(8,128)S(1)} fusion(bf16[24,128,2048]{2,1,0:T(8,128)(2,1)} %param.17), kind=kLoop, calls=%fused_computation.8 | loop fusion | flops 18871296 | bytes 12595200 | tf_op jit(solution)/shard_map/reduce_sum | solution.py:11
  23.1 7.7 %fusion.1 = bf16[3072,2048]{1,0:T(8,128)(2,1)S(1)} fusion(f32[2048]{0:T(1024)S(1)} %copy-done.5, f32[3072]{0:T(1024)S(1)} %rsqrt_bitcast_fusion, bf16[24,128,2048]{2,1,0:T(8,128)(2,1)} %param.17), kind=kLoop, calls=%fused_computation.7 | loop fusion | flops 25165824 | bytes 25186304 | tf_op jit(solution)/shard_map/convert_element_type | solution.py:12
  30.9 4.6 %copy-done.1 = bf16[3072,2048]{1,0:T(8,128)(2,1)} copy-done((bf16[3072,2048]{1,0:T(8,128)(2,1)}, bf16[3072,2048]{1,0:T(8,128)(2,1)S(1)}, u32[]{:S(2)}) %copy-start.1) | copy-done | bytes 12582936
  35.4 4.6 %convolution_convert_fusion.1 = bf16[3072,256]{1,0:T(8,128)(2,1)} fusion(bf16[3072,2048]{1,0:T(8,128)(2,1)S(1)} %fusion.1, bf16[2048,256]{1,0:T(8,128)(2,1)S(1)} %copy-done.9), kind=kOutput, calls=%fused_computation.23 | convolution fusion | flops 3222011904 | bytes 15204352 | tf_op jit(solution)/shard_map/dot_general | solution.py:82
  40.1 5.8 %reshape.253 = bf16[24,128,4,64]{3,2,1,0:T(4,128)(2,1)} reshape(bf16[3072,256]{1,0:T(8,128)(2,1)} %convolution_convert_fusion.1) | data formatting | bytes 3145728 | tf_op jit(solution)/shard_map/reshape | solution.py:85
  45.8 5.3 %copy.135 = bf16[24,128,4,64]{1,3,2,0:T(8,128)(2,1)} copy(bf16[24,128,4,64]{3,2,1,0:T(4,128)(2,1)} %reshape.253) | data formatting | bytes 3145728 | tf_op jit(solution)/shard_map/reshape | solution.py:85
  51.2 1.2 fusion.44
  52.4 4.4 %gather_fusion = bf16[64,128,4,64]{1,3,2,0:T(8,128)(2,1)} fusion(bf16[24,128,4,64]{1,3,2,0:T(8,128)(2,1)} %copy.135, s32[1024]{0:T(1024)S(1)} %pad_clamp_fusion.1), kind=kCustom, calls=%fused_computation | custom fusion | bytes 8388864 | tf_op jit(solution)/shard_map/gather | solution.py:94
  56.8 10.4 %all-to-all-start.1 = ((bf16[64,1,128,4,64]{2,4,3,1,0:T(8,128)(2,1)}), bf16[64,1,128,4,64]{2,4,3,1,0:T(8,128)(2,1)}, u32[]{:S(2)}, u32[]{:S(2)}) async-start(bf16[64,1,128,4,64]{2,4,3,1,0:T(8,128)(2,1)} %bitcast.72), calls=%async_computation.1 | async-start | bytes 8388608 | tf_op jit(solution)/shard_map/all_to_all | solution.py:97
  67.2 9.2 %convolution_convert_fusion = bf16[3072,256]{1,0:T(8,128)(2,1)} fusion(bf16[3072,2048]{1,0:T(8,128)(2,1)} %copy-done.1, bf16[2048,256]{1,0:T(8,128)(2,1)S(1)} %copy-done.10), kind=kOutput, calls=%fused_computation.22 | convolution fusion | flops 3222011904 | bytes 15204352 | tf_op jit(solution)/shard_map/dot_general | solution.py:86
  76.4 5.8 %reshape.254 = bf16[24,128,4,64]{3,2,1,0:T(4,128)(2,1)} reshape(bf16[3072,256]{1,0:T(8,128)(2,1)} %convolution_convert_fusion) | data formatting | bytes 3145728 | tf_op jit(solution)/shard_map/reshape | solution.py:89
  82.1 5.3 %copy.141 = bf16[24,128,4,64]{1,3,2,0:T(8,128)(2,1)} copy(bf16[24,128,4,64]{3,2,1,0:T(4,128)(2,1)} %reshape.254) | data formatting | bytes 3145728 | tf_op jit(solution)/shard_map/reshape | solution.py:89
  87.5 2.6 %fusion.2 = f32[768]{0:T(1024)S(1)} fusion(bf16[768,2048]{1,0:T(8,128)(2,1)} %param.15), kind=kLoop, calls=%fused_computation.11 | loop fusion | flops 4717824 | bytes 3148800 | tf_op jit(solution)/shard_map/reduce_sum | solution.py:11
  90.0 4.5 %gather_fusion.2 = bf16[64,128,4,64]{1,3,2,0:T(8,128)(2,1)} fusion(bf16[24,128,4,64]{1,3,2,0:T(8,128)(2,1)} %copy.141, s32[1024]{0:T(1024)S(1)} %pad_clamp_fusion.1), kind=kCustom, calls=%fused_computation.2 | custom fusion | bytes 8388864 | tf_op jit(solution)/shard_map/gather | solution.py:95
  94.5 23.4 %all-to-all-done.1 = bf16[64,1,128,4,64]{2,4,3,1,0:T(8,128)(2,1)} async-done(((bf16[64,1,128,4,64]{2,4,3,1,0:T(8,128)(2,1)}), bf16[64,1,128,4,64]{2,4,3,1,0:T(8,128)(2,1)}, u32[]{:S(2)}, u32[]{:S(2)}) %all-to-all-start.1) | async-done | bytes 4194336 | tf_op jit(solution)/shard_map/all_to_all | solution.py:97
  117.9 11.6 %all-to-all-start.2 = ((bf16[64,1,128,4,64]{2,4,3,1,0:T(8,128)(2,1)}), bf16[64,1,128,4,64]{2,4,3,1,0:T(8,128)(2,1)}, u32[]{:S(2)}, u32[]{:S(2)}) async-start(bf16[64,1,128,4,64]{2,4,3,1,0:T(8,128)(2,1)} %bitcast.71), calls=%async_computation.2 | async-start | bytes 8388608 | tf_op jit(solution)/shard_map/all_to_all | solution.py:98
  129.5 2.8 %fusion.4 = bf16[768,2048]{1,0:T(8,128)(2,1)S(1)} fusion(bf16[768,2048]{1,0:T(8,128)(2,1)} %param.15, f32[2048]{0:T(1024)S(1)} %copy-done.6, f32[768]{0:T(1024)S(1)} %add_rsqrt_fusion.1), kind=kLoop, calls=%fused_computation.13 | loop fusion | flops 6291456 | bytes 6302720 | tf_op jit(solution)/shard_map/convert_element_type | solution.py:12
  132.3 1.7 copy-done.2
  134.0 1.0 convolution_convert_fusion.3
  135.0 0.3 reshape.204
  135.4 5.6 %fusion.51 = (f32[768]{0:T(1024)S(1)}, f32[768]{0:T(1024)S(1)}, f32[768,256]{1,0:T(8,128)}) fusion(bf16[768,2048]{1,0:T(8,128)(2,1)} %copy-done.2, bf16[2048,256]{1,0:T(8,128)(2,1)} %param.21), kind=kOutput, calls=%fused_computation.108 | convolution fusion | flops 818477568 | bytes 4986880 | tf_op jit(solution)/shard_map/dot_general | solution.py:108
  141.0 2.9 %all-reduce = (f32[768]{0:T(1024)S(1)}, f32[768]{0:T(1024)S(1)}) all-reduce(f32[768]{0:T(1024)S(1)} %get-tuple-element.6, f32[768]{0:T(1024)S(1)} %get-tuple-element.5), channel_id=1, replica_groups=mesh['st'=64,'tp'=2] {'tp'}, use_global_device_ids=true, to_apply=%region_4.5 | all-reduce | flops 1536 | bytes 12288 | tf_op jit(solution)/shard_map/psum | solution.py:111
  143.9 1.4 multiply_convert_fusion
  145.4 1.2 reshape.251
  146.6 2.4 %fusion.16 = f32[6,128,4,64]{1,3,0,2:T(8,128)} fusion(bf16[6,128,4,64]{3,2,1,0:T(4,128)(2,1)} %reshape.251, f32[128,4]{0,1:T(4,128)S(1)} %bitcast.78, bf16[4,128,128]{2,1,0:T(8,128)(2,1)S(1)} %copy-done.4), kind=kOutput, calls=%fused_computation.32 | convolution fusion | flops 50528256 | bytes 1312768 | tf_op jit(solution)/shard_map/hij,njhc->nihc/dot_general | solution.py:120
  149.0 2.4 %copy.152 = f32[6,128,4,64]{3,2,1,0:T(4,128)} copy(f32[6,128,4,64]{1,3,0,2:T(8,128)} %fusion.16) | data formatting | bytes 1572864 | tf_op jit(solution)/shard_map/reshape | solution.py:124
  151.4 3.0 %reshape.252 = f32[768,256]{1,0:T(8,128)} reshape(f32[6,128,4,64]{3,2,1,0:T(4,128)} %copy.152) | data formatting | bytes 1572864 | tf_op jit(solution)/shard_map/reshape | solution.py:124
  154.4 4.0 %fusion.54 = f32[768,256]{1,0:T(8,128)} fusion(bf16[768,2048]{1,0:T(8,128)(2,1)} %copy-done.2, bf16[2048,256]{1,0:T(8,128)(2,1)} %param.20), kind=kOutput, calls=%fused_computation.110 | convolution fusion | flops 805306368 | bytes 4980736 | tf_op jit(solution)/shard_map/dot_general | solution.py:106
  158.4 4.9 %gather_fusion.1 = bf16[48,128,4,64]{1,3,2,0:T(8,128)(2,1)} fusion(bf16[64,128,4,64]{1,3,2,0:T(8,128)(2,1)} %bitcast.11, s32[1024]{0:T(1024)S(1)} %pad_clamp_fusion), kind=kCustom, calls=%fused_computation.1 | custom fusion | bytes 6291648 | tf_op jit(solution)/shard_map/gather | solution.py:102
  163.3 3.8 %bitcast_reduce_fusion = (f32[12,4,64,4]{2,1,3,0:T(4,128)S(1)}, f32[12,4,4,128,64]{3,4,2,1,0:T(8,128)S(1)}) fusion(bf16[12,4,128,4,64]{2,4,3,1,0:T(8,128)(2,1)} %bitcast.73, bf16[12,64,4,64,1]{3,2,1,0,4:T(4,128)(2,1)S(1)} %bitcast.75), kind=kOutput, calls=%fused_computation.17 | convolution fusion | flops 204460032 | bytes 9879552 | tf_op jit(solution)/shard_map/bthe,bplhe->bpthl/dot_general | solution.py:18
  167.1 4.2 %fusion.7 = (bf16[12,4,64,4,128]{4,2,1,3,0:T(8,128)(2,1)}, f32[12,4,64,4]{2,1,3,0:T(4,128)S(1)}) fusion(f32[12,4,4,128,64]{3,4,2,1,0:T(8,128)S(1)} %get-tuple-element.23, f32[12,4,64,4]{2,1,3,0:T(4,128)S(1)} %get-tuple-element.22), kind=kLoop, calls=%fused_computation.20 | loop fusion | flops 6279168 | bytes 9535488 | tf_op jit(solution)/shard_map/convert_element_type | solution.py:26
  171.5 12.2 %all-to-all-done.2 = bf16[64,1,128,4,64]{2,4,3,1,0:T(8,128)(2,1)} async-done(((bf16[64,1,128,4,64]{2,4,3,1,0:T(8,128)(2,1)}), bf16[64,1,128,4,64]{2,4,3,1,0:T(8,128)(2,1)}, u32[]{:S(2)}, u32[]{:S(2)}) %all-to-all-start.2) | async-done | bytes 4194336 | tf_op jit(solution)/shard_map/all_to_all | solution.py:98
  183.7 4.9 %gather_fusion.3 = bf16[48,128,4,64]{1,3,2,0:T(8,128)(2,1)} fusion(bf16[64,128,4,64]{1,3,2,0:T(8,128)(2,1)} %bitcast.17, s32[1024]{0:T(1024)S(1)} %pad_clamp_fusion), kind=kCustom, calls=%fused_computation.3 | custom fusion | bytes 6291648 | tf_op jit(solution)/shard_map/gather | solution.py:103
  188.6 0.1 fusion.53
  188.7 4.8 %multiply_reduce_fusion.1 = f32[12,64,4,64]{1,3,2,0:T(8,128)S(1)} fusion(f32[12,4,64,4]{2,3,1,0:T(4,128)S(1)} %copy.144, f32[12,4,64,4]{2,3,1,0:T(4,128)S(1)} %copy.139, bf16[12,4,128,4,64]{2,4,3,1,0:T(8,128)(2,1)} %bitcast.74, bf16[12,4,64,4,128]{4,2,1,3,0:T(8,128)(2,1)} %get-tuple-element.14), kind=kOutput, calls=%fused_computation.19 | convolution fusion | flops 205062144 | bytes 7176192 | tf_op jit(solution)/shard_map/bpthl,bplhe->bpthe/dot_general | solution.py:24
  193.5 1.3 broadcast_divide_fusion
  194.9 2.7 %copy.145 = f32[12,64,4,64]{3,2,1,0:T(4,128)} copy(f32[12,64,4,64]{1,3,2,0:T(8,128)} %broadcast_divide_fusion) | data formatting | bytes 1572864 | tf_op jit(solution)/shard_map/div | solution.py:39
  197.5 3.0 %div.81 = f32[768,256]{1,0:T(8,128)} reshape(f32[12,64,4,64]{3,2,1,0:T(4,128)} %copy.145) | data formatting | bytes 1572864 | tf_op jit(solution)/shard_map/div | solution.py:39
  200.5 5.2 %fusion.21 = bf16[768,256]{1,0:T(8,128)(2,1)S(1)} fusion(f32[768,256]{1,0:T(8,128)} %div.81, bf16[768,2048]{1,0:T(8,128)(2,1)} %copy-done.2, bf16[2048,256]{1,0:T(8,128)(2,1)} %param.28, f32[768,256]{1,0:T(8,128)S(1)} %copy-done.3, f32[768,256]{1,0:T(8,128)} %fusion.54), kind=kOutput, calls=%fused_computation.37 | convolution fusion | flops 819265536 | bytes 6946816 | tf_op jit(solution)/shard_map/dot_general | solution.py:127
  205.7 0.2 copy.146
  205.9 5.5 %all_to_all.38 = bf16[2,384,256]{1,2,0:T(8,128)(2,1)S(1)} all-to-all(bf16[2,384,256]{1,2,0:T(8,128)(2,1)S(1)} %copy.146), channel_id=1, replica_groups=mesh['st'=64,'tp'=2] {'tp'}, dimensions={0} | all-to-all | bytes 786432 | tf_op jit(solution)/shard_map/all_to_all | solution.py:129
  211.4 2.2 %convolution_convert_fusion.2 = bf16[384,2048]{1,0:T(8,128)(2,1)} fusion(bf16[384,512]{0,1:T(8,128)(2,1)S(1)} %bitcast.76, bf16[512,2048]{1,0:T(8,128)(2,1)S(1)} %copy-done), kind=kOutput, calls=%fused_computation.28 | convolution fusion | flops 806092800 | bytes 4063232 | tf_op jit(solution)/shard_map/dot_general | solution.py:130
  (42 shorter events, 1.1 us)
Async XLA Ops:
  0.0 211.4 %copy-start = (bf16[512,2048]{1,0:T(8,128)(2,1)S(1)}, bf16[512,2048]{1,0:T(8,128)(2,1)}, u32[]{:S(2)}) copy-start(bf16[512,2048]{1,0:T(8,128)(2,1)} %param.29) | copy-start | bytes 6291460
  4.0 47.1 %all-to-all-start = ((s32[64,1,1]{2,1,0:T(1,128)}), s32[64,1,1]{2,1,0:T(1,128)S(1)}, u32[]{:S(2)}, u32[]{:S(2)}) async-start(s32[64,1,1]{2,1,0:T(1,128)} %copy.134), calls=%async_computation | async-start | bytes 65536 | tf_op jit(solution)/shard_map/all_to_all | solution.py:93
  16.0 7.1 %copy-start.5 = (f32[2048]{0:T(1024)S(1)}, f32[2048]{0:T(1024)}, u32[]{:S(2)}) copy-start(f32[2048]{0:T(1024)} %param.19) | copy-start | bytes 24580
  23.1 12.3 %copy-start.9 = (bf16[2048,256]{1,0:T(8,128)(2,1)S(1)}, bf16[2048,256]{1,0:T(8,128)(2,1)}, u32[]{:S(2)}) copy-start(bf16[2048,256]{1,0:T(8,128)(2,1)} %param.26) | copy-start | bytes 3145732
  30.9 4.6 %copy-start.1 = (bf16[3072,2048]{1,0:T(8,128)(2,1)}, bf16[3072,2048]{1,0:T(8,128)(2,1)S(1)}, u32[]{:S(2)}) copy-start(bf16[3072,2048]{1,0:T(8,128)(2,1)S(1)} %fusion.1) | copy-start | bytes 37748740
  56.8 10.4 %copy-start.10 = (bf16[2048,256]{1,0:T(8,128)(2,1)S(1)}, bf16[2048,256]{1,0:T(8,128)(2,1)}, u32[]{:S(2)}) copy-start(bf16[2048,256]{1,0:T(8,128)(2,1)} %param.27) | copy-start | bytes 3145732
  56.8 61.0 %all-to-all-start.1 = ((bf16[64,1,128,4,64]{2,4,3,1,0:T(8,128)(2,1)}), bf16[64,1,128,4,64]{2,4,3,1,0:T(8,128)(2,1)}, u32[]{:S(2)}, u32[]{:S(2)}) async-start(bf16[64,1,128,4,64]{2,4,3,1,0:T(8,128)(2,1)} %bitcast.72), calls=%async_computation.1 | async-start | bytes 8388608 | tf_op jit(solution)/shard_map/all_to_all | solution.py:97
  117.9 11.6 %copy-start.6 = (f32[2048]{0:T(1024)S(1)}, f32[2048]{0:T(1024)}, u32[]{:S(2)}) copy-start(f32[2048]{0:T(1024)} %param.18) | copy-start | bytes 24580
  117.9 65.8 %all-to-all-start.2 = ((bf16[64,1,128,4,64]{2,4,3,1,0:T(8,128)(2,1)}), bf16[64,1,128,4,64]{2,4,3,1,0:T(8,128)(2,1)}, u32[]{:S(2)}, u32[]{:S(2)}) async-start(bf16[64,1,128,4,64]{2,4,3,1,0:T(8,128)(2,1)} %bitcast.71), calls=%async_computation.2 | async-start | bytes 8388608 | tf_op jit(solution)/shard_map/all_to_all | solution.py:98
  129.5 4.5 %copy-start.11 = (bf16[2048,256]{1,0:T(8,128)(2,1)S(1)}, bf16[2048,256]{1,0:T(8,128)(2,1)}, u32[]{:S(2)}) copy-start(bf16[2048,256]{1,0:T(8,128)(2,1)} %param.25) | copy-start | bytes 3145732
  132.3 1.8 copy-start.2
  135.3 8.6 %copy-start.8 = (f32[256]{0:T(256)S(1)}, f32[256]{0:T(256)}, u32[]{:S(2)}) copy-start(f32[256]{0:T(256)} %param.22) | copy-start | bytes 3076
  135.3 11.2 %copy-start.4 = (bf16[4,128,128]{2,1,0:T(8,128)(2,1)S(1)}, bf16[4,128,128]{2,1,0:T(8,128)(2,1)}, u32[]{:S(2)}) copy-start(bf16[4,128,128]{2,1,0:T(8,128)(2,1)} %param.23) | copy-start | bytes 393220
  135.4 11.2 %copy-start.7 = (f32[4,128]{1,0:T(4,128)S(1)}, f32[4,128]{1,0:T(4,128)}, u32[]{:S(2)}) copy-start(f32[4,128]{1,0:T(4,128)} %param.24) | copy-start | bytes 6148
  194.9 5.6 %copy-start.3 = (f32[768,256]{1,0:T(8,128)S(1)}, f32[768,256]{1,0:T(8,128)}, u32[]{:S(2)}) copy-start(f32[768,256]{1,0:T(8,128)} %reshape.252) | copy-start | bytes 2359300
where the time goes:
time: 215 us; the launch traced here: 214 us
  local copies, waits for them, and re-layouts  62.3 us (29%)
  matrix products  42.8 us (20%)
  waiting for transfers between devices  35.5 us (17%)
  starting transfers between devices  33.9 us (16%)
  other arithmetic  30.3 us (14%)
  blocking collectives  8.41 us (4%)
    all_to_all x1, waiting for transfers between devices, per_device(): lax.all_to_all(sent_keys, 'st', split_axis=0, concat_axis=0, tiled=True)  23.4 us
    all_to_all x1, waiting for transfers between devices, per_device(): lax.all_to_all(sent_values, 'st', split_axis=0, concat_axis=0, tiled=True)  12.2 us
    all_to_all x1, starting transfers between devices, per_device(): lax.all_to_all(slot_local, 'st', split_axis=0, concat_axis=0, tiled=True)  12 us
    all_to_all x1, starting transfers between devices, per_device(): lax.all_to_all(sent_values, 'st', split_axis=0, concat_axis=0, tiled=True)  11.6 us
    reshape x2, local copies, waits for them, and re-layouts, per_device(): store_values.reshape(store_count, passage_length, local_heads, head_dim)  11.1 us
    reshape x2, local copies, waits for them, and re-layouts, per_device(): store_keys.reshape(store_count, passage_length, local_heads, head_dim)  11.1 us
    convert_element_type x2, other arithmetic, rms_scaled(): return (scaled * gain_vector).astype(jnp.bfloat16)  10.5 us
    all_to_all x1, starting transfers between devices, per_device(): lax.all_to_all(sent_keys, 'st', split_axis=0, concat_axis=0, tiled=True)  10.4 us
  transfers between devices with their start and end apart: 3, of which 2 were waited for; matrix products, arithmetic and copies ran while one was open for 45% of the time, Pallas kernels for 0%

commit v1 on v0

v1 whole, which is shorter than its diff:
```python
import functools

import jax
import jax.numpy as jnp
from jax import lax
from jax.experimental import pallas as pl
from jax.experimental.pallas import tpu as pltpu
from jax.sharding import PartitionSpec as P

norm_eps = 1e-06
MESH = pl.DeviceIdType.MESH
SIDE = 4
N_ST = SIDE**3
GROUP = 4


def rms_scaled(matrix, gain_vector):
    values = matrix.astype(jnp.float32)
    scaled = values * lax.rsqrt(jnp.mean(values * values, axis=-1, keepdims=True) + norm_eps)
    return (scaled * gain_vector).astype(jnp.bfloat16)


def torus_shift(index, offset, sign):
    total = 0
    for unit in (1, SIDE, SIDE * SIDE):
        mine = lax.rem(lax.div(index, unit), SIDE)
        away = lax.rem(lax.div(offset, unit), SIDE)
        total = total + lax.rem(mine + (away if sign > 0 else SIDE - away), SIDE) * unit
    return total


def step_offset(step):
    return lax.rem(step * 27, N_ST)


def exchange_kernel(
    owner_ref,
    span_ref,
    local_ref,
    head_mask_ref,
    query_ref,
    key_ref,
    value_ref,
    memory_ref,
    slots,
    asked,
    parts,
    back,
    logs,
    back_logs,
    table,
    table_smem,
    send_query,
    recv_query,
    send_table,
    recv_table,
    send_part,
    recv_part,
    send_log,
    recv_log,
    local_sem,
):
    me = lax.axis_index("st")
    core = lax.axis_index("tp")
    span_length = slots.shape[1]
    width = slots.shape[2]
    head_dim = width // head_mask_ref.shape[0]
    span_count = memory_ref.shape[0]
    pick_count = owner_ref.shape[0] // span_count
    barrier = pltpu.get_barrier_semaphore()

    def greet(step, carry):
        pl.semaphore_signal(
            barrier,
            inc=1,
            device_id=(torus_shift(me, step_offset(step), 1), core),
            device_id_type=MESH,
        )
        return carry

    lax.fori_loop(1, N_ST, greet, 0)

    def fill(slot, carry):
        slots[slot] = query_ref[span_ref[slot]]
        return carry

    lax.fori_loop(0, N_ST, fill, 0)
    table[me] = local_ref[...]
    pl.semaphore_wait(barrier, N_ST - 1)

    def table_copy(peer):
        return pltpu.make_async_remote_copy(
            src_ref=local_ref,
            dst_ref=table.at[me],
            send_sem=send_table,
            recv_sem=recv_table,
            device_id=(peer, core),
            device_id_type=MESH,
        )

    def query_copy(peer):
        return pltpu.make_async_remote_copy(
            src_ref=slots.at[peer],
            dst_ref=asked.at[me],
            send_sem=send_query,
            recv_sem=recv_query.at[me],
            device_id=(peer, core),
            device_id_type=MESH,
        )

    def send_tables(step, carry):
        table_copy(torus_shift(me, step_offset(step), 1)).start()
        return carry

    lax.fori_loop(1, N_ST, send_tables, 0)

    def send_queries(step, carry):
        query_copy(torus_shift(me, step_offset(step), 1)).start()
        return carry

    lax.fori_loop(1, N_ST, send_queries, 0)
    asked[me] = slots[me]
    rest = pl.ds(0, N_ST - 1)
    pltpu.make_async_copy(table.at[rest], table.at[rest], recv_table).wait()
    copy = pltpu.make_async_copy(table, table_smem, local_sem)
    copy.start()
    copy.wait()

    def attend(source):
        index = table_smem[source, 0, me]
        keys = key_ref[index]
        values_t = value_ref[index]
        query = asked[source]
        spread = jnp.concatenate(
            [query * head_mask_ref[h] for h in range(head_mask_ref.shape[0])], axis=0
        )
        scores = lax.dot_general(
            keys, spread, (((1,), (1,)), ((), ())), preferred_element_type=jnp.float32
        ) * (head_dim**-0.5)
        peak = jnp.max(scores, axis=0, keepdims=True)
        weights = jnp.exp(scores - peak)
        total = jnp.sum(weights, axis=0, keepdims=True)
        summed = jnp.dot(values_t, weights.astype(jnp.bfloat16), preferred_element_type=jnp.float32)
        lane_head = lax.broadcasted_iota(jnp.int32, (head_dim, width), 1) // head_dim
        mine = summed[:head_dim]
        for h in range(1, head_mask_ref.shape[0]):
            mine = jnp.where(lane_head == h, summed[h * head_dim : (h + 1) * head_dim], mine)
        return (mine / total).astype(jnp.bfloat16), peak + jnp.log(total)

    def part_copy(source):
        return pltpu.make_async_remote_copy(
            src_ref=parts.at[source],
            dst_ref=back.at[me],
            send_sem=send_part,
            recv_sem=recv_part,
            device_id=(source, core),
            device_id_type=MESH,
        )

    def log_copy(source):
        return pltpu.make_async_remote_copy(
            src_ref=logs.at[source],
            dst_ref=back_logs.at[me],
            send_sem=send_log,
            recv_sem=recv_log,
            device_id=(source, core),
            device_id_type=MESH,
        )

    def send_back(step):
        source = torus_shift(me, step_offset(step), -1)
        part_copy(source).start()
        log_copy(source).start()

    def serve(group, carry):
        for j in range(GROUP):
            step = group * GROUP + j
            source = torus_shift(me, step_offset(step), -1)

            @pl.when(step > 0)
            def _():
                pltpu.make_async_copy(asked.at[source], asked.at[source], recv_query.at[source]).wait()

        for j in range(GROUP):
            step = group * GROUP + j
            source = torus_shift(me, step_offset(step), -1)
            part, log_total = attend(source)
            parts[source] = part
            logs[source] = log_total

        for j in range(GROUP):
            step = (group - 1) * GROUP + j

            @pl.when(step > 0)
            def _():
                send_back(step)

        return carry

    lax.fori_loop(0, N_ST // GROUP, serve, 0)
    for j in range(GROUP):
        send_back(N_ST - GROUP + j)
    back[me] = parts[me]
    back_logs[me] = logs[me]
    pltpu.make_async_copy(back.at[rest], back.at[rest], recv_part).wait()
    pltpu.make_async_copy(back_logs.at[rest], back_logs.at[rest], recv_log).wait()

    def merge(span, carry):
        owners = [owner_ref[span * pick_count + k] for k in range(pick_count)]
        levels = [back_logs[o] for o in owners]
        top = functools.reduce(jnp.maximum, levels)
        scales = [jnp.exp(level - top) for level in levels]
        total = functools.reduce(jnp.add, scales)
        summed = functools.reduce(
            jnp.add, [s * back[o].astype(jnp.float32) for s, o in zip(scales, owners)]
        )
        turned = (summed / total).T
        memory_ref[span] = jnp.concatenate(
            [turned[h * span_length : (h + 1) * span_length] for h in range(head_mask_ref.shape[0])],
            axis=1,
        )
        return carry

    lax.fori_loop(0, span_count, merge, 0)
    pltpu.make_async_copy(slots.at[rest], slots.at[rest], send_query).wait()
    pltpu.make_async_copy(table.at[rest], table.at[rest], send_table).wait()
    pltpu.make_async_copy(parts.at[rest], parts.at[rest], send_part).wait()
    pltpu.make_async_copy(logs.at[rest], logs.at[rest], send_log).wait()


def exchange(owner, slot_span, slot_local, queries, keys, values_t):
    span_count, span_length, width = queries.shape
    head_dim = values_t.shape[1] // 4
    heads = width // head_dim
    lanes = jnp.arange(width, dtype=jnp.int32) // head_dim
    head_mask = (lanes[None, None, :] == jnp.arange(heads, dtype=jnp.int32)[:, None, None]).astype(
        jnp.bfloat16
    )
    head_mask = jnp.broadcast_to(head_mask, (heads, span_length, width))
    block = pltpu.VMEM((N_ST, span_length, width), jnp.bfloat16)
    smem = pl.BlockSpec(memory_space=pltpu.SMEM)
    vmem = pl.BlockSpec(memory_space=pltpu.VMEM)
    return pl.pallas_call(
        exchange_kernel,
        out_shape=jax.ShapeDtypeStruct((span_count, span_length, width), jnp.float32),
        in_specs=[smem, smem] + [vmem] * 5,
        out_specs=vmem,
        scratch_shapes=[block] * 4
        + [pltpu.VMEM((N_ST, 1, width), jnp.float32)] * 2
        + [
            pltpu.VMEM((N_ST, 1, 128), jnp.int32),
            pltpu.SMEM((N_ST, 1, 128), jnp.int32),
            pltpu.SemaphoreType.DMA,
            pltpu.SemaphoreType.DMA((N_ST,)),
        ]
        + [pltpu.SemaphoreType.DMA] * 7,
        compiler_params=pltpu.CompilerParams(
            collective_id=0, has_side_effects=True, vmem_limit_bytes=40 << 20
        ),
    )(owner, slot_span, slot_local, head_mask, queries, keys, values_t)


def per_device(
    tokens,
    route_ids,
    store,
    token_gain,
    store_gain,
    carry_weight,
    spatial_weight,
    spatial_gain,
    position_mix,
    position_bias,
    query_weight,
    key_weight,
    read_weight,
    blend_weight,
    output_weight,
):
    row_count = tokens.shape[0]
    local_heads = position_mix.shape[0]
    block_length = position_mix.shape[1]
    local_width = carry_weight.shape[1]
    head_dim = local_width // local_heads
    span_count, pick_count = route_ids.shape
    span_length = row_count // span_count
    store_count, passage_length = (store.shape[0], store.shape[1])
    flat_ids = route_ids.reshape(-1)
    owner = flat_ids // store_count
    hit = owner[:, None] == jnp.arange(128, dtype=jnp.int32)[None, :]
    span_of = jnp.arange(span_count * pick_count, dtype=jnp.int32)[:, None] // pick_count
    slot_span = jnp.sum(jnp.where(hit, span_of, 0), axis=0)
    slot_local = jnp.sum(jnp.where(hit, (flat_ids % store_count)[:, None], 0), axis=0)
    store_rows = rms_scaled(store.reshape(store_count * passage_length, store.shape[2]), store_gain)
    keys = jnp.dot(store_rows, key_weight, preferred_element_type=jnp.float32).astype(jnp.bfloat16)
    keys = keys.reshape(store_count, passage_length, local_width)
    values = jnp.dot(store_rows, read_weight, preferred_element_type=jnp.float32).astype(jnp.bfloat16)
    values_t = values.reshape(store_count, passage_length, local_width).transpose(0, 2, 1)
    normed = rms_scaled(tokens, token_gain)
    queries = jnp.dot(normed, query_weight, preferred_element_type=jnp.float32).astype(jnp.bfloat16)
    queries = queries.reshape(span_count, span_length, local_width)
    memory = exchange(owner, slot_span, slot_local.reshape(1, 128), queries, keys, values_t)
    memory = memory.reshape(row_count, local_width)
    carry_branch = jnp.dot(normed, carry_weight, preferred_element_type=jnp.float32)
    spatial = jax.nn.gelu(
        jnp.dot(normed, spatial_weight, preferred_element_type=jnp.float32), approximate=False
    )
    total_width = local_width * lax.axis_size("tp")
    moment_one, moment_two = lax.psum(
        (jnp.sum(spatial, axis=1), jnp.sum(spatial * spatial, axis=1)), "tp"
    )
    channel_mean = (moment_one / total_width)[:, None]
    channel_spread = (moment_two / total_width)[:, None] - channel_mean * channel_mean
    spatial_in = (
        (spatial - channel_mean) * lax.rsqrt(channel_spread + norm_eps) * spatial_gain
    ).astype(jnp.bfloat16)
    blocks = spatial_in.reshape(row_count // block_length, block_length, local_heads, head_dim)
    mixed_blocks = jnp.einsum(
        "hij,njhc->nihc", position_mix, blocks, preferred_element_type=jnp.float32
    )
    mixed_blocks = mixed_blocks + position_bias.T[None, :, :, None]
    gated_mix = jax.nn.gelu(carry_branch, approximate=False) * mixed_blocks.reshape(
        row_count, local_width
    )
    blend_gate = jax.nn.sigmoid(jnp.dot(normed, blend_weight, preferred_element_type=jnp.float32))
    mixed_rows = (gated_mix + blend_gate * memory).astype(jnp.bfloat16)
    by_rows = lax.all_to_all(mixed_rows, "tp", split_axis=0, concat_axis=1, tiled=True)
    return jnp.dot(by_rows, output_weight, preferred_element_type=jnp.float32).astype(jnp.bfloat16)


def solution(mesh):
    in_specs = (
        P("st", None),
        P("st", None),
        P("st", None, None),
        P(),
        P(),
        P(None, "tp"),
        P(None, "tp"),
        P("tp"),
        P("tp", None, None),
        P("tp", None),
        P(None, "tp"),
        P(None, "tp"),
        P(None, "tp"),
        P(None, "tp"),
        P(),
    )
    out_specs = P(("st", "tp"), None)
    return jax.shard_map(
        per_device, mesh=mesh, in_specs=in_specs, out_specs=out_specs, check_vma=False
    )
```

time: 215 us -> 131 us (0.61)
  Pallas kernels: 0 us -> 63.5 us
  local copies, waits for them, and re-layouts: 62.3 us -> 12 us
  waiting for transfers between devices: 35.5 us -> 0 us
  starting transfers between devices: 33.9 us -> 0 us
  matrix products: 42.8 us -> 23.3 us
  other arithmetic: 30.3 us -> 22.9 us
    pallas_call x0 -> x1, Pallas kernels: none -> 63.5 us  [exchange(): pl.pallas_call(exchange_kernel, out_shape=jax.ShapeDtypeStruct((span_coun...]
    all_to_all x3 -> x0, waiting for transfers between devices: 35.5 us -> none  [the longest x1 23.4 us: per_device(): lax.all_to_all(sent_keys, 'st', split_axis=0, concat_axis=0, tiled=True)]
    all_to_all x3 -> x0, starting transfers between devices: 33.9 us -> none  [the longest x1 12 us: per_device(): lax.all_to_all(slot_local, 'st', split_axis=0, concat_axis=0, tiled=True)]
    reshape x5 -> x1, local copies, waits for them, and re-layouts: 22.5 us -> 2.59 us  [per_device(): values.reshape(store_count, passage_length, local_width).transpose(0, 2, 1)]
    gather x4 -> x0, local copies, waits for them, and re-layouts: 18.7 us -> none  [the longest x1 4.92 us: per_device(): span_values = got_values.reshape(slot_shape)[position].reshape(span_shape)]
    dot_general x2 -> x0, matrix products: 8.58 us -> none  [the longest x1 4.77 us: passage_partial(): jnp.einsum('bpthl,bplhe->bpthe', weights.astype(jnp.bfloat16), value_rows...]
    div x5 -> x2, local copies, waits for them, and re-layouts: 5.88 us -> 0.18 us  [per_device(): owner = flat_ids // store_count]
    unnamed x24 -> x30, local copies, waits for them, and re-layouts: 6.36 us -> 1.08 us
  transfers between devices with their start and end apart: 3 -> 0, of which waited for: 2 -> 0; matrix products, arithmetic and copies ran while one was open for 45% -> 0% of each run, Pallas kernels for 0% -> 0%
where the time goes in v1:
time: 131 us; the launch traced here: 130 us
  Pallas kernels  63.5 us (48%)
  matrix products  23.3 us (18%)
  other arithmetic  22.9 us (17%)
  local copies, waits for them, and re-layouts  12 us (9%)
  blocking collectives  8.34 us (6%)
    pallas_call x1, Pallas kernels, exchange(): pl.pallas_call(exchange_kernel, out_shape=jax.ShapeDtypeStruct((span_coun...  63.5 us
    convert_element_type x2, other arithmetic, rms_scaled(): return (scaled * gain_vector).astype(jnp.bfloat16)  10.5 us
    reduce_sum x2, other arithmetic, rms_scaled(): jnp.mean(values * values, axis=-1, keepdims=True) + norm_eps  9.66 us
    all_to_all x1, blocking collectives, per_device(): lax.all_to_all(mixed_rows, 'tp', split_axis=0, concat_axis=1, tiled=True)  4.81 us
    reshape x2, local copies, waits for them, and re-layouts, per_device(): mixed_blocks.reshape(row_count, local_width)  4.74 us
    dot_general x1, matrix products, per_device(): jnp.dot(store_rows, key_weight, preferred_element_type=jnp.float32)  4.65 us
    dot_general x1, matrix products, per_device(): jnp.dot(store_rows, read_weight, preferred_element_type=jnp.float32)  4.62 us
    psum x1, blocking collectives, per_device(): lax.psum((jnp.sum(spatial, axis=1), jnp.sum(spatial * spatial, axis=1)),...  3.53 us

profile of v1, /device:TPU:1, one launch (start us, length us, event | category | flops | bytes accessed | tf_op | source)
XLA Modules:
  0.0 130.3 jit_solution(17107334821458486786)
XLA Ops:
  0.0 0.0 copy-start
  0.0 0.8 broadcast_remainder_fusion
  0.8 0.7 sign_compare_fusion
  1.5 0.1 copy.41
  1.6 0.1 rem.42
  1.7 0.1 copy.42
  1.8 0.1 div.56
  1.9 0.1 copy.40
  2.0 0.1 ne.90
  2.1 2.6 %fusion.2 = f32[768]{0:T(1024)S(1)} fusion(bf16[768,2048]{1,0:T(8,128)(2,1)} %param.15), kind=kLoop, calls=%fused_computation.6 | loop fusion | flops 4717824 | bytes 3148800 | tf_op jit(solution)/shard_map/reduce_sum | solution.py:19
  4.7 0.0 copy-start.6
  4.7 7.1 %multiply_reduce_fusion = f32[24,128]{1,0:T(8,128)S(1)} fusion(bf16[24,128,2048]{2,1,0:T(8,128)(2,1)} %param.17), kind=kLoop, calls=%fused_computation.3 | loop fusion | flops 18871296 | bytes 12595200 | tf_op jit(solution)/shard_map/reduce_sum | solution.py:19
  11.8 0.0 copy-done.6
  11.8 0.0 copy-start.10
  11.8 7.7 %fusion.1 = bf16[3072,2048]{1,0:T(8,128)(2,1)S(1)} fusion(f32[2048]{0:T(1024)S(1)} %copy-done.6, f32[3072]{0:T(1024)S(1)} %rsqrt_bitcast_fusion, bf16[24,128,2048]{2,1,0:T(8,128)(2,1)} %param.17), kind=kLoop, calls=%fused_computation.2 | loop fusion | flops 25165824 | bytes 25186304 | tf_op jit(solution)/shard_map/convert_element_type | solution.py:20
  19.6 0.0 copy-done.10
  19.6 0.0 copy-start.11
  19.6 4.7 %convolution_convert_fusion.1 = bf16[3072,256]{1,0:T(8,128)(2,1)} fusion(bf16[3072,2048]{1,0:T(8,128)(2,1)S(1)} %fusion.1, bf16[2048,256]{1,0:T(8,128)(2,1)S(1)} %copy-done.10), kind=kOutput, calls=%fused_computation.10 | convolution fusion | flops 3222011904 | bytes 15204352 | tf_op jit(solution)/shard_map/dot_general | solution.py:295
  24.2 0.0 copy-done.11
  24.2 4.6 %convolution_convert_fusion = bf16[3072,256]{1,0:T(8,128)(2,1)} fusion(bf16[3072,2048]{1,0:T(8,128)(2,1)S(1)} %fusion.1, bf16[2048,256]{1,0:T(8,128)(2,1)S(1)} %copy-done.11), kind=kOutput, calls=%fused_computation.9 | convolution fusion | flops 3222011904 | bytes 15204352 | tf_op jit(solution)/shard_map/dot_general | solution.py:297
  28.9 2.6 %copy.43 = bf16[24,128,256]{1,2,0:T(8,128)(2,1)} copy(bf16[24,128,256]{2,1,0:T(8,128)(2,1)} %bitcast.47) | data formatting | bytes 3145728 | tf_op jit(solution)/shard_map/reshape | solution.py:298
  31.5 0.0 copy-done.7
  31.5 2.8 %fusion.4 = bf16[768,2048]{1,0:T(8,128)(2,1)S(1)} fusion(bf16[768,2048]{1,0:T(8,128)(2,1)} %param.15, f32[2048]{0:T(1024)S(1)} %copy-done.7, f32[768]{0:T(1024)S(1)} %add_rsqrt_fusion.1), kind=kLoop, calls=%fused_computation.8 | loop fusion | flops 6291456 | bytes 6302720 | tf_op jit(solution)/shard_map/convert_element_type | solution.py:20
  34.2 0.0 copy-done.12
  34.2 0.0 copy-start.3
  34.3 0.0 copy-start.13
  34.3 1.0 convolution_convert_fusion.3
  35.3 0.7 copy-done.3
  35.9 0.4 copy-done.13
  36.3 2.9 %fusion.34 = (f32[768]{0:T(1024)S(1)}, f32[768]{0:T(1024)S(1)}, f32[768,256]{1,0:T(8,128)S(1)}) fusion(bf16[768,2048]{1,0:T(8,128)(2,1)S(1)} %fusion.4, bf16[2048,256]{1,0:T(8,128)(2,1)S(1)} %copy-done.13), kind=kOutput, calls=%fused_computation.85 | convolution fusion | flops 818477568 | bytes 4986880 | tf_op jit(solution)/shard_map/dot_general | solution.py:306
  39.2 3.5 %all-reduce = (f32[768]{0:T(1024)S(1)}, f32[768]{0:T(1024)S(1)}) all-reduce(f32[768]{0:T(1024)S(1)} %get-tuple-element.6, f32[768]{0:T(1024)S(1)} %get-tuple-element.5), channel_id=1, replica_groups=mesh['st'=64,'tp'=2] {'tp'}, use_global_device_ids=true, to_apply=%region_4.5 | all-reduce | flops 1536 | bytes 12288 | tf_op jit(solution)/shard_map/psum | solution.py:309
  42.7 1.0 multiply_convert_fusion
  43.8 1.8 %reshape.178 = bf16[6,128,4,64]{3,2,1,0:T(4,128)(2,1)S(1)} reshape(bf16[768,256]{1,0:T(8,128)(2,1)} %multiply_convert_fusion) | data formatting | bytes 786432 | tf_op jit(solution)/shard_map/reshape | solution.py:317
  45.6 0.0 copy-done.5
  45.6 0.0 copy-done.8
  45.6 1.3 fusion.6
  46.9 2.5 %copy.49 = f32[6,128,4,64]{3,2,1,0:T(4,128)} copy(f32[6,128,4,64]{1,3,0,2:T(8,128)} %fusion.6) | data formatting | bytes 1572864 | tf_op jit(solution)/shard_map/reshape | solution.py:322
  49.4 2.2 %reshape.179 = f32[768,256]{1,0:T(8,128)S(1)} reshape(f32[6,128,4,64]{3,2,1,0:T(4,128)} %copy.49) | data formatting | bytes 1572864 | tf_op jit(solution)/shard_map/reshape | solution.py:322
  51.7 0.0 copy-start.2
  51.7 3.3 %fusion.36 = f32[768,256]{1,0:T(8,128)S(1)} fusion(bf16[768,2048]{1,0:T(8,128)(2,1)} %copy-done.3, bf16[2048,256]{1,0:T(8,128)(2,1)} %param.20), kind=kOutput, calls=%fused_computation.86 | convolution fusion | flops 805306368 | bytes 4980736 | tf_op jit(solution)/shard_map/dot_general | solution.py:304
  55.0 0.0 copy-start.4
  55.0 0.0 copy-start.14
  55.0 0.1 select_reduce_fusion
  55.2 63.5 %shard_map.145 = f32[12,64,256]{2,1,0:T(8,128)S(1)} custom-call(s32[48]{0:T(128)S(1)} %get-tuple-element.17.owner_ref, s32[128]{0:T(128)S(1)} %get-tuple-element.8.span_ref, s32[1,128]{1,0:T(1,128)S(1)} %bitcast.46, bf16[4,64,256]{2,1,0:T(8,128)(2,1)S(1)} %broadcast_in_dim.23.head_mask_ref, bf16[12,64,256]{2,1,0:T(8,128)(2,1)S(1)} %bitcast.45, ...), custom_call_target="tpu_custom_call" | custom-call | tf_op jit(solution)/shard_map/pallas_call | solution.py:243
  118.7 3.4 %fusion.11 = bf16[768,256]{1,0:T(8,128)(2,1)} fusion(f32[768,256]{1,0:T(8,128)S(1)} %bitcast.44, bf16[768,2048]{1,0:T(8,128)(2,1)S(1)} %copy-done.4, bf16[2048,256]{1,0:T(8,128)(2,1)S(1)} %copy-done.14, f32[768,256]{1,0:T(8,128)S(1)} %reshape.179, f32[768,256]{1,0:T(8,128)S(1)} %fusion.36), kind=kOutput, calls=%fused_computation.20 | convolution fusion | flops 819265536 | bytes 6946816 | tf_op jit(solution)/shard_map/dot_general | solution.py:325
  122.1 1.2 copy.44
  123.3 4.8 %all_to_all.19 = bf16[2,384,256]{1,2,0:T(8,128)(2,1)S(1)} all-to-all(bf16[2,384,256]{1,2,0:T(8,128)(2,1)S(1)} %copy.44), channel_id=1, replica_groups=mesh['st'=64,'tp'=2] {'tp'}, dimensions={0} | all-to-all | bytes 786432 | tf_op jit(solution)/shard_map/all_to_all | solution.py:327
  128.1 2.2 %convolution_convert_fusion.2 = bf16[384,2048]{1,0:T(8,128)(2,1)} fusion(bf16[384,512]{0,1:T(8,128)(2,1)S(1)} %bitcast.48, bf16[512,2048]{1,0:T(8,128)(2,1)S(1)} %copy-done), kind=kOutput, calls=%fused_computation.11 | convolution fusion | flops 806092800 | bytes 4063232 | tf_op jit(solution)/shard_map/dot_general | solution.py:328
  (19 shorter events, 0.1 us)
Async XLA Ops:
  0.0 128.1 %copy-start = (bf16[512,2048]{1,0:T(8,128)(2,1)S(1)}, bf16[512,2048]{1,0:T(8,128)(2,1)}, u32[]{:S(2)}) copy-start(bf16[512,2048]{1,0:T(8,128)(2,1)} %param.29) | copy-start | bytes 6291460
  4.7 7.1 %copy-start.6 = (f32[2048]{0:T(1024)S(1)}, f32[2048]{0:T(1024)}, u32[]{:S(2)}) copy-start(f32[2048]{0:T(1024)} %param.19) | copy-start | bytes 24580
  11.8 7.7 %copy-start.10 = (bf16[2048,256]{1,0:T(8,128)(2,1)S(1)}, bf16[2048,256]{1,0:T(8,128)(2,1)}, u32[]{:S(2)}) copy-start(bf16[2048,256]{1,0:T(8,128)(2,1)} %param.26) | copy-start | bytes 3145732
  19.6 4.7 %copy-start.11 = (bf16[2048,256]{1,0:T(8,128)(2,1)S(1)}, bf16[2048,256]{1,0:T(8,128)(2,1)}, u32[]{:S(2)}) copy-start(bf16[2048,256]{1,0:T(8,128)(2,1)} %param.27) | copy-start | bytes 3145732
  28.9 2.6 %copy-start.7 = (f32[2048]{0:T(1024)S(1)}, f32[2048]{0:T(1024)}, u32[]{:S(2)}) copy-start(f32[2048]{0:T(1024)} %param.18) | copy-start | bytes 24580
  31.5 2.8 %copy-start.12 = (bf16[2048,256]{1,0:T(8,128)(2,1)S(1)}, bf16[2048,256]{1,0:T(8,128)(2,1)}, u32[]{:S(2)}) copy-start(bf16[2048,256]{1,0:T(8,128)(2,1)} %param.25) | copy-start | bytes 3145732
  34.2 1.7 %copy-start.3 = (bf16[768,2048]{1,0:T(8,128)(2,1)}, bf16[768,2048]{1,0:T(8,128)(2,1)S(1)}, u32[]{:S(2)}) copy-start(bf16[768,2048]{1,0:T(8,128)(2,1)S(1)} %fusion.4) | copy-start | bytes 9437188
  34.3 2.0 %copy-start.13 = (bf16[2048,256]{1,0:T(8,128)(2,1)S(1)}, bf16[2048,256]{1,0:T(8,128)(2,1)}, u32[]{:S(2)}) copy-start(bf16[2048,256]{1,0:T(8,128)(2,1)} %param.21) | copy-start | bytes 3145732
  36.3 6.5 %copy-start.9 = (f32[256]{0:T(256)S(1)}, f32[256]{0:T(256)}, u32[]{:S(2)}) copy-start(f32[256]{0:T(256)} %param.22) | copy-start | bytes 3076
  36.3 9.3 %copy-start.5 = (bf16[4,128,128]{2,1,0:T(8,128)(2,1)S(1)}, bf16[4,128,128]{2,1,0:T(8,128)(2,1)}, u32[]{:S(2)}) copy-start(bf16[4,128,128]{2,1,0:T(8,128)(2,1)} %param.23) | copy-start | bytes 393220
  36.3 9.4 %copy-start.8 = (f32[4,128]{1,0:T(4,128)S(1)}, f32[4,128]{1,0:T(4,128)}, u32[]{:S(2)}) copy-start(f32[4,128]{1,0:T(4,128)} %param.24) | copy-start | bytes 6148
  51.7 3.5 %copy-start.1 = (bf16[24,128,256]{1,2,0:T(8,128)(2,1)S(1)}, bf16[24,128,256]{1,2,0:T(8,128)(2,1)}, u32[]{:S(2)}) copy-start(bf16[24,128,256]{1,2,0:T(8,128)(2,1)} %copy.43) | copy-start | bytes 4718596
  51.7 3.5 %copy-start.2 = (bf16[3072,256]{1,0:T(8,128)(2,1)S(1)}, bf16[3072,256]{1,0:T(8,128)(2,1)}, u32[]{:S(2)}) copy-start(bf16[3072,256]{1,0:T(8,128)(2,1)} %convolution_convert_fusion.1) | copy-start | bytes 4718596
  55.0 63.7 %copy-start.4 = (bf16[768,2048]{1,0:T(8,128)(2,1)S(1)}, bf16[768,2048]{1,0:T(8,128)(2,1)}, u32[]{:S(2)}) copy-start(bf16[768,2048]{1,0:T(8,128)(2,1)} %copy-done.3) | copy-start | bytes 9437188
  55.0 63.7 %copy-start.14 = (bf16[2048,256]{1,0:T(8,128)(2,1)S(1)}, bf16[2048,256]{1,0:T(8,128)(2,1)}, u32[]{:S(2)}) copy-start(bf16[2048,256]{1,0:T(8,128)(2,1)} %param.28) | copy-start | bytes 3145732

commit v2 on v1

v2 whole, which is shorter than its diff:
```python
import functools

import jax
import jax.numpy as jnp
from jax import lax
from jax.experimental import pallas as pl
from jax.experimental.pallas import tpu as pltpu
from jax.sharding import PartitionSpec as P

norm_eps = 1e-06
MESH = pl.DeviceIdType.MESH
SIDE = 4
N_ST = SIDE**3
GROUP = 4
CHUNK = 16
TILE = 256


def torus_shift(index, offset, sign):
    total = 0
    for unit in (1, SIDE, SIDE * SIDE):
        mine = lax.rem(lax.div(index, unit), SIDE)
        away = lax.rem(lax.div(offset, unit), SIDE)
        total = total + lax.rem(mine + (away if sign > 0 else SIDE - away), SIDE) * unit
    return total


def step_offset(step):
    return lax.rem(step * 27, N_ST)


def gelu(x):
    return 0.5 * x * (1.0 + lax.erf(x * 0.5**0.5))


def norm_rows(source, target, gain_ref, count, source_base, target_base):
    features = source.shape[1]
    gain = gain_ref[...]

    def some(i, carry):
        rows = pl.ds(pl.multiple_of(source_base + i * CHUNK, CHUNK), CHUNK)
        values = source[rows, :].astype(jnp.float32)
        mean = jnp.sum(values * values, axis=1, keepdims=True) * (1.0 / features)
        scaled = values * lax.rsqrt(mean + norm_eps) * gain
        rows = pl.ds(pl.multiple_of(target_base + i * CHUNK, CHUNK), CHUNK)
        target[rows, :] = scaled.astype(jnp.bfloat16)
        return carry

    lax.fori_loop(0, count // CHUNK, some, 0, unroll=4)


def layer_kernel(
    ids_smem,
    ids_ref,
    tokens_hbm,
    store_hbm,
    token_gain_hbm,
    store_gain_hbm,
    carry_weight_hbm,
    spatial_weight_hbm,
    spatial_gain_hbm,
    position_mix_hbm,
    position_bias_hbm,
    query_weight_hbm,
    key_weight_hbm,
    read_weight_hbm,
    blend_weight_hbm,
    out_ref,
    tokens,
    store,
    token_gain,
    store_gain,
    carry_weight,
    spatial_weight,
    spatial_gain,
    position_mix,
    position_bias,
    query_weight,
    key_weight,
    read_weight,
    blend_weight,
    rows_normed,
    head_mask,
    queries,
    keys,
    values_t,
    slots,
    asked,
    parts,
    back,
    logs,
    back_logs,
    span_row,
    span_smem,
    local_row,
    table,
    table_smem,
    gated,
    spatial,
    blend,
    moments,
    other_moments,
    mixed,
    other_mixed,
    load_tokens,
    load_store,
    load_small,
    send_query,
    recv_query,
    send_table,
    recv_table,
    send_part,
    recv_part,
    send_log,
    recv_log,
    send_moments,
    recv_moments,
    send_mixed,
    recv_mixed,
    span_sem,
    table_sem,
):
    me = lax.axis_index("st")
    core = lax.axis_index("tp")
    span_count, pick_count = ids_ref.shape
    span_length, width = slots.shape[1:]
    passage_count, passage_length = keys.shape[:2]
    heads, block_length = position_bias.shape
    head_dim = width // heads
    row_count = tokens.shape[0]
    half = row_count // 2
    barrier = pltpu.get_barrier_semaphore()

    def greet(step, carry):
        pl.semaphore_signal(
            barrier,
            inc=1,
            device_id=(torus_shift(me, step_offset(step), 1), core),
            device_id_type=MESH,
        )
        return carry

    lax.fori_loop(1, N_ST, greet, 0)
    pl.semaphore_signal(barrier, inc=1, device_id=(me, 1 - core), device_id_type=MESH)

    def tile_rows(i, size):
        return pl.ds(pl.multiple_of(i * size, size), size)

    def token_load(i):
        rows = tile_rows(i, TILE)
        return pltpu.make_async_copy(tokens_hbm.at[rows], tokens.at[rows], load_tokens.at[i])

    def store_load(i):
        rows = tile_rows(i, TILE)
        return pltpu.make_async_copy(store_hbm.at[rows], store.at[rows], load_store.at[i])

    small = {}
    for n, (name, source, target) in enumerate(
        (
            ("token_gain", token_gain_hbm, token_gain),
            ("query_weight", query_weight_hbm, query_weight),
            ("store_gain", store_gain_hbm, store_gain),
            ("key_weight", key_weight_hbm, key_weight),
            ("read_weight", read_weight_hbm, read_weight),
            ("spatial_weight", spatial_weight_hbm, spatial_weight),
            ("spatial_gain", spatial_gain_hbm, spatial_gain),
            ("carry_weight", carry_weight_hbm, carry_weight),
            ("blend_weight", blend_weight_hbm, blend_weight),
            ("position_mix", position_mix_hbm, position_mix),
            ("position_bias", position_bias_hbm, position_bias),
        )
    ):
        small[name] = pltpu.make_async_copy(source, target, load_small.at[n])
    small["token_gain"].start()
    token_tiles = row_count // TILE
    store_tiles = store.shape[0] // TILE
    for i in range(token_tiles):
        token_load(i).start()
    small["query_weight"].start()
    small["store_gain"].start()
    small["key_weight"].start()
    small["read_weight"].start()
    for i in range(store_tiles):
        store_load(i).start()
    for name in (
        "spatial_weight",
        "spatial_gain",
        "carry_weight",
        "blend_weight",
        "position_mix",
        "position_bias",
    ):
        small[name].start()

    ids = ids_ref[...]
    lane = lax.broadcasted_iota(jnp.int32, (span_count, 128), 1) * passage_count
    span_index = lax.broadcasted_iota(jnp.int32, (span_count, 128), 0)
    slot_span = jnp.zeros((span_count, 128), jnp.int32)
    slot_local = jnp.zeros((span_count, 128), jnp.int32)
    for k in range(pick_count):
        local = ids[:, k : k + 1] - lane
        hit = (local >= 0) & (local < passage_count)
        slot_span = slot_span + jnp.where(hit, span_index, 0)
        slot_local = slot_local + jnp.where(hit, local, 0)
    slot_span = jnp.sum(slot_span, axis=0, keepdims=True)
    slot_local = jnp.sum(slot_local, axis=0, keepdims=True)
    span_row[...] = jnp.minimum(slot_span, span_count - 1)
    local_row[...] = jnp.minimum(slot_local, passage_count - 1)
    table[me] = local_row[...]
    mask_lane = lax.broadcasted_iota(jnp.int32, (span_length, width), 1) // head_dim
    for h in range(heads):
        head_mask[h] = jnp.where(mask_lane == h, 1.0, 0.0).astype(jnp.bfloat16)
    span_copy = pltpu.make_async_copy(span_row, span_smem, span_sem)
    span_copy.start()

    small["token_gain"].wait()

    def token_norm(i, carry):
        token_load(i).wait()
        norm_rows(tokens, tokens, token_gain, TILE, i * TILE, i * TILE)
        return carry

    lax.fori_loop(0, token_tiles, token_norm, 0)
    small["query_weight"].wait()

    def token_query(i, carry):
        found = jnp.dot(
            tokens[tile_rows(i, TILE), :], query_weight[...], preferred_element_type=jnp.float32
        ).astype(jnp.bfloat16)
        spans = TILE // span_length
        for s in range(spans):
            queries[i * spans + s] = found[s * span_length : (s + 1) * span_length]
        return carry

    lax.fori_loop(0, token_tiles, token_query, 0)
    span_copy.wait()

    def fill(slot, carry):
        slots[slot] = queries[span_smem[0, slot]]
        return carry

    lax.fori_loop(0, N_ST, fill, 0, unroll=4)
    pl.semaphore_wait(barrier, N_ST)

    def table_copy(peer):
        return pltpu.make_async_remote_copy(
            src_ref=local_row,
            dst_ref=table.at[me],
            send_sem=send_table,
            recv_sem=recv_table,
            device_id=(peer, core),
            device_id_type=MESH,
        )

    def query_copy(peer):
        return pltpu.make_async_remote_copy(
            src_ref=slots.at[peer],
            dst_ref=asked.at[me],
            send_sem=send_query,
            recv_sem=recv_query.at[me],
            device_id=(peer, core),
            device_id_type=MESH,
        )

    def send_tables(step, carry):
        table_copy(torus_shift(me, step_offset(step), 1)).start()
        return carry

    lax.fori_loop(1, N_ST, send_tables, 0)

    def send_queries(step, carry):
        query_copy(torus_shift(me, step_offset(step), 1)).start()
        return carry

    lax.fori_loop(1, N_ST, send_queries, 0)
    asked[me] = slots[me]

    small["store_gain"].wait()
    small["key_weight"].wait()
    small["read_weight"].wait()

    def project(i, carry):
        store_load(i).wait()
        norm_rows(store, rows_normed, store_gain, TILE, i * TILE, 0)
        rows = rows_normed[...]
        key_rows = jnp.dot(rows, key_weight[...], preferred_element_type=jnp.float32)
        value_rows = jnp.dot(rows, read_weight[...], preferred_element_type=jnp.float32)
        several = TILE // passage_length
        for p in range(several):
            part = slice(p * passage_length, (p + 1) * passage_length)
            keys[i * several + p] = key_rows[part].astype(jnp.bfloat16)
            values_t[i * several + p] = value_rows[part].T.astype(jnp.bfloat16)
        return carry

    lax.fori_loop(0, store_tiles, project, 0)

    rest = pl.ds(0, N_ST - 1)
    pltpu.make_async_copy(table.at[rest], table.at[rest], recv_table).wait()
    table_read = pltpu.make_async_copy(table, table_smem, table_sem)
    table_read.start()
    table_read.wait()

    def attend(source):
        index = table_smem[source, 0, me]
        query = asked[source]
        spread = jnp.concatenate([query * head_mask[h] for h in range(heads)], axis=0)
        scores = lax.dot_general(
            keys[index], spread, (((1,), (1,)), ((), ())), preferred_element_type=jnp.float32
        ) * (head_dim**-0.5)
        peak = jnp.max(scores, axis=0, keepdims=True)
        weights = jnp.exp(scores - peak)
        total = jnp.sum(weights, axis=0, keepdims=True)
        summed = jnp.dot(
            values_t[index], weights.astype(jnp.bfloat16), preferred_element_type=jnp.float32
        )
        mine = summed[:head_dim]
        for h in range(1, heads):
            mine = jnp.where(mask_lane == h, summed[h * head_dim : (h + 1) * head_dim], mine)
        return (mine / total).astype(jnp.bfloat16), peak + jnp.log(total)

    def part_copy(source):
        return pltpu.make_async_remote_copy(
            src_ref=parts.at[source],
            dst_ref=back.at[me],
            send_sem=send_part,
            recv_sem=recv_part,
            device_id=(source, core),
            device_id_type=MESH,
        )

    def log_copy(source):
        return pltpu.make_async_remote_copy(
            src_ref=logs.at[source],
            dst_ref=back_logs.at[me],
            send_sem=send_log,
            recv_sem=recv_log,
            device_id=(source, core),
            device_id_type=MESH,
        )

    def send_back(step):
        source = torus_shift(me, step_offset(step), -1)
        part_copy(source).start()
        log_copy(source).start()

    def serve(group, carry):
        for j in range(GROUP):
            step = group * GROUP + j
            source = torus_shift(me, step_offset(step), -1)

            @pl.when(step > 0)
            def _():
                pltpu.make_async_copy(asked.at[source], asked.at[source], recv_query.at[source]).wait()

        for j in range(GROUP):
            source = torus_shift(me, step_offset(group * GROUP + j), -1)
            part, log_total = attend(source)
            parts[source] = part
            logs[source] = log_total

        for j in range(GROUP):
            step = (group - 1) * GROUP + j

            @pl.when(step > 0)
            def _():
                send_back(step)

        return carry

    lax.fori_loop(0, N_ST // GROUP, serve, 0)
    for j in range(GROUP):
        send_back(N_ST - GROUP + j)
    back[me] = parts[me]
    back_logs[me] = logs[me]

    small["spatial_weight"].wait()
    moment_lane = lax.broadcasted_iota(jnp.int32, (TILE, 128), 1)

    def spatial_tile(i, carry):
        rows = tile_rows(i, TILE)
        found = gelu(
            jnp.dot(tokens[rows, :], spatial_weight[...], preferred_element_type=jnp.float32)
        )
        spatial[rows, :] = found
        one = jnp.sum(found, axis=1, keepdims=True)
        two = jnp.sum(found * found, axis=1, keepdims=True)
        moments[rows, :] = jnp.where(moment_lane < 64, one, two)
        return carry

    lax.fori_loop(0, token_tiles, spatial_tile, 0)
    small["carry_weight"].wait()
    small["blend_weight"].wait()

    def carry_tile(i, carry):
        rows = tile_rows(i, TILE)
        gated[rows, :] = gelu(
            jnp.dot(tokens[rows, :], carry_weight[...], preferred_element_type=jnp.float32)
        )
        blend[rows, :] = jax.nn.sigmoid(
            jnp.dot(tokens[rows, :], blend_weight[...], preferred_element_type=jnp.float32)
        )
        return carry

    moment_copy = pltpu.make_async_remote_copy(
        src_ref=moments,
        dst_ref=other_moments,
        send_sem=send_moments,
        recv_sem=recv_moments,
        device_id=(me, 1 - core),
        device_id_type=MESH,
    )
    moment_copy.start()
    lax.fori_loop(0, token_tiles, carry_tile, 0)
    small["spatial_gain"].wait()
    small["position_mix"].wait()
    small["position_bias"].wait()
    moment_copy.wait()
    block_head = lax.broadcasted_iota(jnp.int32, (block_length, width), 1) // head_dim
    bias_columns = jnp.concatenate([position_bias[...]] * (8 // heads), axis=0).T
    bias = jnp.zeros((block_length, width), jnp.float32)
    for h in range(heads):
        bias = jnp.where(block_head == h, bias_columns[:, h : h + 1], bias)

    def mix_block(i, carry):
        rows = tile_rows(i, block_length)
        both = (moments[rows, :] + other_moments[rows, :]) * (0.5 / width)
        mean = both[:, :1]
        spread = both[:, 64:65] - mean * mean
        fed = (
            (spatial[rows, :] - mean) * lax.rsqrt(spread + norm_eps) * spatial_gain[...]
        ).astype(jnp.bfloat16)
        every = jnp.dot(position_mix[...], fed, preferred_element_type=jnp.float32)
        found = every[:block_length]
        for h in range(1, heads):
            found = jnp.where(
                block_head == h, every[h * block_length : (h + 1) * block_length], found
            )
        gated[rows, :] = gated[rows, :] * (found + bias)
        return carry

    lax.fori_loop(0, row_count // block_length, mix_block, 0)

    pltpu.make_async_copy(back.at[rest], back.at[rest], recv_part).wait()
    pltpu.make_async_copy(back_logs.at[rest], back_logs.at[rest], recv_log).wait()

    def merge(span):
        owners = [lax.div(ids_smem[span, k], passage_count) for k in range(pick_count)]
        levels = [back_logs[o] for o in owners]
        top = functools.reduce(jnp.maximum, levels)
        scales = [jnp.exp(level - top) for level in levels]
        total = functools.reduce(jnp.add, scales)
        summed = functools.reduce(
            jnp.add, [s * back[o].astype(jnp.float32) for s, o in zip(scales, owners)]
        )
        turned = (summed / total).T
        memory = jnp.concatenate(
            [turned[h * span_length : (h + 1) * span_length] for h in range(heads)], axis=1
        )
        rows = tile_rows(span, span_length)
        mixed[rows, :] = (gated[rows, :] + blend[rows, :] * memory).astype(jnp.bfloat16)

    def merge_half(first):
        def some(i, carry):
            merge(first + 2 * i)
            merge(first + 2 * i + 1)
            return carry

        lax.fori_loop(0, span_count // 4, some, 0)

    merge_half((1 - core) * (span_count // 2))
    mixed_copy = pltpu.make_async_remote_copy(
        src_ref=mixed.at[tile_rows(1 - core, half)],
        dst_ref=other_mixed,
        send_sem=send_mixed,
        recv_sem=recv_mixed,
        device_id=(me, 1 - core),
        device_id_type=MESH,
    )
    mixed_copy.start()
    merge_half(core * (span_count // 2))
    mine = tile_rows(core, half)

    @pl.when(core == 0)
    def _():
        out_ref[:, :width] = mixed[mine, :]

    @pl.when(core == 1)
    def _():
        out_ref[:, width:] = mixed[mine, :]

    mixed_copy.wait()

    @pl.when(core == 0)
    def _():
        out_ref[:, width:] = other_mixed[...]

    @pl.when(core == 1)
    def _():
        out_ref[:, :width] = other_mixed[...]

    pltpu.make_async_copy(slots.at[rest], slots.at[rest], send_query).wait()
    pltpu.make_async_copy(table.at[rest], table.at[rest], send_table).wait()
    pltpu.make_async_copy(parts.at[rest], parts.at[rest], send_part).wait()
    pltpu.make_async_copy(logs.at[rest], logs.at[rest], send_log).wait()


def per_device(
    tokens,
    route_ids,
    store,
    token_gain,
    store_gain,
    carry_weight,
    spatial_weight,
    spatial_gain,
    position_mix,
    position_bias,
    query_weight,
    key_weight,
    read_weight,
    blend_weight,
    output_weight,
):
    row_count, features = tokens.shape
    heads, block_length = position_mix.shape[:2]
    width = carry_weight.shape[1]
    span_count = route_ids.shape[0]
    span_length = row_count // span_count
    passage_count, passage_length = store.shape[:2]
    store = store.reshape(passage_count * passage_length, features)
    token_gain = token_gain.reshape(1, features)
    store_gain = store_gain.reshape(1, features)
    spatial_gain = spatial_gain.reshape(1, width)
    position_mix = position_mix.reshape(heads * block_length, block_length)
    bf16, f32 = jnp.bfloat16, jnp.float32
    block = pltpu.VMEM((N_ST, span_length, width), bf16)
    weight = pltpu.VMEM((features, width), bf16)
    by_row = pltpu.VMEM((row_count, width), f32)
    dma = pltpu.SemaphoreType.DMA
    anywhere = pl.BlockSpec(memory_space=pl.ANY)
    by_rows = pl.pallas_call(
        layer_kernel,
        out_shape=jax.ShapeDtypeStruct((row_count // 2, 2 * width), bf16),
        in_specs=[
            pl.BlockSpec(memory_space=pltpu.SMEM),
            pl.BlockSpec(memory_space=pltpu.VMEM),
        ]
        + [anywhere] * 13,
        out_specs=pl.BlockSpec(memory_space=pltpu.VMEM),
        scratch_shapes=[
            pltpu.VMEM(tokens.shape, bf16),
            pltpu.VMEM(store.shape, bf16),
            pltpu.VMEM((1, features), f32),
            pltpu.VMEM((1, features), f32),
            weight,
            weight,
            pltpu.VMEM((1, width), f32),
            pltpu.VMEM(position_mix.shape, bf16),
            pltpu.VMEM(position_bias.shape, f32),
            weight,
            weight,
            weight,
            weight,
            pltpu.VMEM((TILE, features), bf16),
            pltpu.VMEM((heads, span_length, width), bf16),
            pltpu.VMEM((span_count, span_length, width), bf16),
            pltpu.VMEM((passage_count, passage_length, width), bf16),
            pltpu.VMEM((passage_count, width, passage_length), bf16),
            block,
            block,
            block,
            block,
            pltpu.VMEM((N_ST, 1, width), f32),
            pltpu.VMEM((N_ST, 1, width), f32),
            pltpu.VMEM((1, 128), jnp.int32),
            pltpu.SMEM((1, 128), jnp.int32),
            pltpu.VMEM((1, 128), jnp.int32),
            pltpu.VMEM((N_ST, 1, 128), jnp.int32),
            pltpu.SMEM((N_ST, 1, 128), jnp.int32),
            by_row,
            by_row,
            by_row,
            pltpu.VMEM((row_count, 128), f32),
            pltpu.VMEM((row_count, 128), f32),
            pltpu.VMEM((row_count, width), bf16),
            pltpu.VMEM((row_count // 2, width), bf16),
            dma((row_count // TILE,)),
            dma((store.shape[0] // TILE,)),
            dma((11,)),
            dma,
            dma((N_ST,)),
        ]
        + [dma] * 12,
        compiler_params=pltpu.CompilerParams(
            collective_id=0, has_side_effects=True, vmem_limit_bytes=60 << 20
        ),
    )(
        route_ids,
        route_ids,
        tokens,
        store,
        token_gain,
        store_gain,
        carry_weight,
        spatial_weight,
        spatial_gain,
        position_mix,
        position_bias,
        query_weight,
        key_weight,
        read_weight,
        blend_weight,
    )
    return jnp.dot(by_rows, output_weight, preferred_element_type=f32).astype(bf16)


def solution(mesh):
    in_specs = (
        P("st", None),
        P("st", None),
        P("st", None, None),
        P(),
        P(),
        P(None, "tp"),
        P(None, "tp"),
        P("tp"),
        P("tp", None, None),
        P("tp", None),
        P(None, "tp"),
        P(None, "tp"),
        P(None, "tp"),
        P(None, "tp"),
        P(),
    )
    out_specs = P(("st", "tp"), None)
    return jax.shard_map(
        per_device, mesh=mesh, in_specs=in_specs, out_specs=out_specs, check_vma=False
    )
```

time: 131 us -> 81.9 us (0.63)
  other arithmetic: 22.9 us -> 0 us
  matrix products: 23.3 us -> 3.12 us
  Pallas kernels: 63.5 us -> 77 us
  local copies, waits for them, and re-layouts: 12 us -> 1.51 us
  blocking collectives: 8.34 us -> 0 us
    dot_general x8 -> x1, matrix products: 23.3 us -> 3.12 us  [per_device(): jnp.dot(by_rows, output_weight, preferred_element_type=f32).astype(bf16)]
    pallas_call x1, Pallas kernels: 63.5 us -> 77 us  [per_device(): pl.pallas_call(layer_kernel, out_shape=jax.ShapeDtypeStruct((row_count //...]
    convert_element_type x4 -> x0, other arithmetic: 11.5 us -> none  [the longest x2 10.5 us: rms_scaled(): return (scaled * gain_vector).astype(jnp.bfloat16)]
    reduce_sum x3 -> x0, other arithmetic: 9.76 us -> none  [the longest x2 9.66 us: rms_scaled(): jnp.mean(values * values, axis=-1, keepdims=True) + norm_eps]
    reshape x4 -> x0, local copies, waits for them, and re-layouts: 9.15 us -> none  [the longest x2 4.74 us: per_device(): mixed_blocks.reshape(row_count, local_width)]
    all_to_all x1 -> x0, blocking collectives: 4.81 us -> none  [per_device(): lax.all_to_all(mixed_rows, 'tp', split_axis=0, concat_axis=1, tiled=True)]
    psum x1 -> x0, blocking collectives: 3.53 us -> none  [per_device(): lax.psum((jnp.sum(spatial, axis=1), jnp.sum(spatial * spatial, axis=1)),...]
where the time goes in v2:
time: 81.9 us; the launch traced here: 81.7 us
  Pallas kernels  77 us (94%)
  matrix products  3.12 us (4%)
  local copies, waits for them, and re-layouts  1.51 us (2%)
    pallas_call x1, Pallas kernels, per_device(): pl.pallas_call(layer_kernel, out_shape=jax.ShapeDtypeStruct((row_count //...  77 us
    dot_general x1, matrix products, per_device(): jnp.dot(by_rows, output_weight, preferred_element_type=f32).astype(bf16)  3.12 us

profile of v2, /device:TPU:1, one launch (start us, length us, event | category | flops | bytes accessed | tf_op | source)
XLA Modules:
  0.0 81.7 jit_solution(504845641926987137)
XLA Ops:
  0.0 0.0 copy-start
  0.0 1.5 %copy.16.ids_smem.ids_ref = s32[12,4]{1,0:T(8,128)} copy(s32[12,4]{0,1:T(4,128)} %param.16) | data formatting | bytes 384 | tf_op args[1]
  1.5 77.0 %shard_map.145 = bf16[384,512]{1,0:T(8,128)(2,1)} custom-call(s32[12,4]{1,0:T(8,128)} %copy.16.ids_smem.ids_ref, s32[12,4]{1,0:T(8,128)} %copy.16.ids_smem.ids_ref, bf16[768,2048]{1,0:T(8,128)(2,1)} %tokens_hbm.1, bf16[3072,2048]{1,0:T(8,128)(2,1)} %bitcast.7, f32[1,2048]{1,0:T(1,128)} %bitcast.9, f32[1,2048]{1,0:T(1,128)} %bitcast.10, ...), custom_call_target="tpu_custom_call" | custom-call | tf_op jit(solution)/shard_map/pallas_call | solution.py:541
  78.6 0.0 copy-done
  78.6 3.1 %convolution_convert_fusion = bf16[384,2048]{1,0:T(8,128)(2,1)} fusion(bf16[384,512]{1,0:T(8,128)(2,1)} %shard_map.145, bf16[512,2048]{1,0:T(8,128)(2,1)S(1)} %copy-done), kind=kOutput, calls=%fused_computation | convolution fusion | flops 806092800 | bytes 4063232 | tf_op jit(solution)/shard_map/dot_general | solution.py:614
Async XLA Ops:
  0.0 78.6 %copy-start = (bf16[512,2048]{1,0:T(8,128)(2,1)S(1)}, bf16[512,2048]{1,0:T(8,128)(2,1)}, u32[]{:S(2)}) copy-start(bf16[512,2048]{1,0:T(8,128)(2,1)} %param.29) | copy-start | bytes 6291460

commit v3 on v2

--- a/solution.py
+++ b/solution.py
@@ -16,24 +16,19 @@
 TILE = 256
 
 
-def torus_shift(index, offset, sign):
-    total = 0
-    for unit in (1, SIDE, SIDE * SIDE):
-        mine = lax.rem(lax.div(index, unit), SIDE)
-        away = lax.rem(lax.div(offset, unit), SIDE)
-        total = total + lax.rem(mine + (away if sign > 0 else SIDE - away), SIDE) * unit
-    return total
-
-
-def step_offset(step):
-    return lax.rem(step * 27, N_ST)
+OFFSETS = [
+    ((b + j) % SIDE, (a + j) % SIDE, j)
+    for a in range(SIDE)
+    for b in range(SIDE)
+    for j in range(SIDE)
+]
 
 
 def gelu(x):
     return 0.5 * x * (1.0 + lax.erf(x * 0.5**0.5))
 
 
-def norm_rows(source, target, gain_ref, count, source_base, target_base):
+def norm_rows(source, target, gain_ref, count, source_base, target_base, unroll=4):
     features = source.shape[1]
     gain = gain_ref[...]
 
@@ -46,7 +41,7 @@
         target[rows, :] = scaled.astype(jnp.bfloat16)
         return carry
 
-    lax.fori_loop(0, count // CHUNK, some, 0, unroll=4)
+    lax.fori_loop(0, count // CHUNK, some, 0, unroll=unroll)
 
 
 def layer_kernel(
@@ -90,6 +85,7 @@
     back,
     logs,
     back_logs,
+    ids_square,
     span_row,
     span_smem,
     local_row,
@@ -122,25 +118,32 @@
 ):
     me = lax.axis_index("st")
     core = lax.axis_index("tp")
-    span_count, pick_count = ids_ref.shape
+    pick_count, span_count = ids_ref.shape
     span_length, width = slots.shape[1:]
     passage_count, passage_length = keys.shape[:2]
     heads, block_length = position_bias.shape
     head_dim = width // heads
     row_count = tokens.shape[0]
     half = row_count // 2
+    my_z, my_y, my_x = lax.div(me, SIDE * SIDE), lax.rem(lax.div(me, SIDE), SIDE), lax.rem(me, SIDE)
+    ahead = [
+        [lax.rem(digit + d, SIDE) * unit for d in range(SIDE)]
+        for digit, unit in ((my_z, SIDE * SIDE), (my_y, SIDE), (my_x, 1))
+    ]
+    peers = [ahead[0][dz] + ahead[1][dy] + ahead[2][dx] for dz, dy, dx in OFFSETS]
+
+    def sources(group):
+        a, b = lax.div(group, SIDE), lax.rem(group, SIDE)
+        return [
+            lax.rem(my_z - b - j + 2 * SIDE, SIDE) * (SIDE * SIDE)
+            + lax.rem(my_y - a - j + 2 * SIDE, SIDE) * SIDE
+            + lax.rem(my_x - j + SIDE, SIDE)
+            for j in range(GROUP)
+        ]
+
     barrier = pltpu.get_barrier_semaphore()
-
-    def greet(step, carry):
-        pl.semaphore_signal(
-            barrier,
-            inc=1,
-            device_id=(torus_shift(me, step_offset(step), 1), core),
-            device_id_type=MESH,
-        )
-        return carry
-
-    lax.fori_loop(1, N_ST, greet, 0)
+    for peer in peers[1:]:
+        pl.semaphore_signal(barrier, inc=1, device_id=(peer, core), device_id_type=MESH)
     pl.semaphore_signal(barrier, inc=1, device_id=(me, 1 - core), device_id_type=MESH)
 
     def tile_rows(i, size):
@@ -192,7 +195,9 @@
     ):
         small[name].start()
 
-    ids = ids_ref[...]
+    ids_square[...] = jnp.zeros_like(ids_square)
+    ids_square[:pick_count, :span_count] = ids_ref[...].astype(jnp.float32)
+    ids = ids_square[...].T[:span_count].astype(jnp.int32)
     lane = lax.broadcasted_iota(jnp.int32, (span_count, 128), 1) * passage_count
     span_index = lax.broadcasted_iota(jnp.int32, (span_count, 128), 0)
     slot_span = jnp.zeros((span_count, 128), jnp.int32)
@@ -215,24 +220,22 @@
 
     small["token_gain"].wait()
 
-    def token_norm(i, carry):
-        token_load(i).wait()
-        norm_rows(tokens, tokens, token_gain, TILE, i * TILE, i * TILE)
-        return carry
-
-    lax.fori_loop(0, token_tiles, token_norm, 0)
-    small["query_weight"].wait()
-
-    def token_query(i, carry):
+    def token_query(i):
         found = jnp.dot(
-            tokens[tile_rows(i, TILE), :], query_weight[...], preferred_element_type=jnp.float32
+            tokens[i * TILE : (i + 1) * TILE, :], query_weight[...], preferred_element_type=jnp.float32
         ).astype(jnp.bfloat16)
         spans = TILE // span_length
         for s in range(spans):
             queries[i * spans + s] = found[s * span_length : (s + 1) * span_length]
-        return carry
-
-    lax.fori_loop(0, token_tiles, token_query, 0)
+
+    for i in range(token_tiles):
+        token_load(i).wait()
+        if i == 1:
+            small["query_weight"].wait()
+        norm_rows(tokens, tokens, token_gain, TILE, i * TILE, i * TILE, TILE // CHUNK if i else 4)
+        if i:
+            token_query(i - 1)
+    token_query(token_tiles - 1)
     span_copy.wait()
 
     def fill(slot, carry):
@@ -262,17 +265,10 @@
             device_id_type=MESH,
         )
 
-    def send_tables(step, carry):
-        table_copy(torus_shift(me, step_offset(step), 1)).start()
-        return carry
-
-    lax.fori_loop(1, N_ST, send_tables, 0)
-
-    def send_queries(step, carry):
-        query_copy(torus_shift(me, step_offset(step), 1)).start()
-        return carry
-
-    lax.fori_loop(1, N_ST, send_queries, 0)
+    for peer in peers[1:]:
+        table_copy(peer).start()
+    for peer in peers[1:]:
+        query_copy(peer).start()
     asked[me] = slots[me]
 
     small["store_gain"].wait()
@@ -338,38 +334,34 @@
             device_id_type=MESH,
         )
 
-    def send_back(step):
-        source = torus_shift(me, step_offset(step), -1)
+    def send_back(source):
         part_copy(source).start()
         log_copy(source).start()
 
     def serve(group, carry):
-        for j in range(GROUP):
-            step = group * GROUP + j
-            source = torus_shift(me, step_offset(step), -1)
-
-            @pl.when(step > 0)
-            def _():
+        now = sources(group)
+        for j, source in enumerate(now):
+
+            @pl.when(group + j > 0)
+            def _(source=source):
                 pltpu.make_async_copy(asked.at[source], asked.at[source], recv_query.at[source]).wait()
 
-        for j in range(GROUP):
-            source = torus_shift(me, step_offset(group * GROUP + j), -1)
+        for source in now:
             part, log_total = attend(source)
             parts[source] = part
             logs[source] = log_total
 
-        for j in range(GROUP):
-            step = (group - 1) * GROUP + j
-
-            @pl.when(step > 0)
-            def _():
-                send_back(step)
+        for j, source in enumerate(sources(group - 1)):
+
+            @pl.when((group > 1) | ((group == 1) & (j > 0)))
+            def _(source=source):
+                send_back(source)
 
         return carry
 
     lax.fori_loop(0, N_ST // GROUP, serve, 0)
-    for j in range(GROUP):
-        send_back(N_ST - GROUP + j)
+    for source in sources(N_ST // GROUP - 1):
+        send_back(source)
     back[me] = parts[me]
     back_logs[me] = logs[me]
 
@@ -444,7 +436,7 @@
     pltpu.make_async_copy(back_logs.at[rest], back_logs.at[rest], recv_log).wait()
 
     def merge(span):
-        owners = [lax.div(ids_smem[span, k], passage_count) for k in range(pick_count)]
+        owners = [lax.div(ids_smem[k, span], passage_count) for k in range(pick_count)]
         levels = [back_logs[o] for o in owners]
         top = functools.reduce(jnp.maximum, levels)
         scales = [jnp.exp(level - top) for level in levels]
@@ -572,6 +564,7 @@
             block,
             pltpu.VMEM((N_ST, 1, width), f32),
             pltpu.VMEM((N_ST, 1, width), f32),
+            pltpu.VMEM((8, 128), f32),
             pltpu.VMEM((1, 128), jnp.int32),
             pltpu.SMEM((1, 128), jnp.int32),
             pltpu.VMEM((1, 128), jnp.int32),
@@ -595,8 +588,8 @@
             collective_id=0, has_side_effects=True, vmem_limit_bytes=60 << 20
         ),
     )(
-        route_ids,
-        route_ids,
+        route_ids.T,
+        route_ids.T,
         tokens,
         store,
         token_gain,

time: 81.9 us -> 74.8 us (0.913)
  Pallas kernels: 77 us -> 71.5 us
  local copies, waits for them, and re-layouts: 1.51 us -> 0.01 us
    pallas_call x1, Pallas kernels: 77 us -> 71.5 us  [per_device(): pl.pallas_call(layer_kernel, out_shape=jax.ShapeDtypeStruct((row_count //...]
    unnamed x3 -> x2, local copies, waits for them, and re-layouts: 1.51 us -> 0.01 us
where the time goes in v3:
time: 74.8 us; the launch traced here: 74.7 us
  Pallas kernels  71.5 us (96%)
  matrix products  3.12 us (4%)
    pallas_call x1, Pallas kernels, per_device(): pl.pallas_call(layer_kernel, out_shape=jax.ShapeDtypeStruct((row_count //...  71.5 us
    dot_general x1, matrix products, per_device(): jnp.dot(by_rows, output_weight, preferred_element_type=f32).astype(bf16)  3.12 us

profile of v3, /device:TPU:1, one launch (start us, length us, event | category | flops | bytes accessed | tf_op | source)
XLA Modules:
  0.0 74.7 jit_solution(16533955718360644412)
XLA Ops:
  0.0 0.0 copy-start
  0.0 71.5 %shard_map.145 = bf16[384,512]{1,0:T(8,128)(2,1)} custom-call(s32[4,12]{1,0:T(4,128)} %bitcast.12, s32[4,12]{1,0:T(4,128)} %bitcast.13, bf16[768,2048]{1,0:T(8,128)(2,1)} %tokens_hbm.1, bf16[3072,2048]{1,0:T(8,128)(2,1)} %bitcast.8, f32[1,2048]{1,0:T(1,128)} %bitcast.10, f32[1,2048]{1,0:T(1,128)} %bitcast.11, bf16[2048,256]{1,0:T(8,128)(2,1)} %carry_weight_hbm.1, ...), custom_call_target="tpu_custom_call" | custom-call | tf_op jit(solution)/shard_map/pallas_call | solution.py:533
  71.5 0.0 copy-done
  71.5 3.1 %convolution_convert_fusion = bf16[384,2048]{1,0:T(8,128)(2,1)} fusion(bf16[384,512]{1,0:T(8,128)(2,1)} %shard_map.145, bf16[512,2048]{1,0:T(8,128)(2,1)S(1)} %copy-done), kind=kOutput, calls=%fused_computation | convolution fusion | flops 806092800 | bytes 4063232 | tf_op jit(solution)/shard_map/dot_general | solution.py:607
Async XLA Ops:
  0.0 71.5 %copy-start = (bf16[512,2048]{1,0:T(8,128)(2,1)S(1)}, bf16[512,2048]{1,0:T(8,128)(2,1)}, u32[]{:S(2)}) copy-start(bf16[512,2048]{1,0:T(8,128)(2,1)} %param.29) | copy-start | bytes 6291460

commit v4 on v3

--- a/solution.py
+++ b/solution.py
@@ -97,7 +97,6 @@
     moments,
     other_moments,
     mixed,
-    other_mixed,
     load_tokens,
     load_store,
     load_small,
@@ -124,7 +123,6 @@
     heads, block_length = position_bias.shape
     head_dim = width // heads
     row_count = tokens.shape[0]
-    half = row_count // 2
     my_z, my_y, my_x = lax.div(me, SIDE * SIDE), lax.rem(lax.div(me, SIDE), SIDE), lax.rem(me, SIDE)
     ahead = [
         [lax.rem(digit + d, SIDE) * unit for d in range(SIDE)]
@@ -180,20 +178,22 @@
     for i in range(token_tiles):
         token_load(i).start()
     small["query_weight"].start()
-    small["store_gain"].start()
-    small["key_weight"].start()
-    small["read_weight"].start()
-    for i in range(store_tiles):
-        store_load(i).start()
-    for name in (
-        "spatial_weight",
-        "spatial_gain",
-        "carry_weight",
-        "blend_weight",
-        "position_mix",
-        "position_bias",
-    ):
-        small[name].start()
+
+    def start_later_loads():
+        small["store_gain"].start()
+        small["key_weight"].start()
+        small["read_weight"].start()
+        for i in range(store_tiles):
+            store_load(i).start()
+        for name in (
+            "spatial_weight",
+            "spatial_gain",
+            "carry_weight",
+            "blend_weight",
+            "position_mix",
+            "position_bias",
+        ):
+            small[name].start()
 
     ids_square[...] = jnp.zeros_like(ids_square)
     ids_square[:pick_count, :span_count] = ids_ref[...].astype(jnp.float32)
@@ -230,11 +230,13 @@
 
     for i in range(token_tiles):
         token_load(i).wait()
-        if i == 1:
+        if i == token_tiles - 1:
             small["query_weight"].wait()
-        norm_rows(tokens, tokens, token_gain, TILE, i * TILE, i * TILE, TILE // CHUNK if i else 4)
-        if i:
-            token_query(i - 1)
+            start_later_loads()
+        norm_rows(tokens, tokens, token_gain, TILE, i * TILE, i * TILE, TILE // CHUNK if i == token_tiles - 1 else 4)
+        if i == token_tiles - 1:
+            for k in range(i):
+                token_query(k)
     token_query(token_tiles - 1)
     span_copy.wait()
 
@@ -449,47 +451,47 @@
             [turned[h * span_length : (h + 1) * span_length] for h in range(heads)], axis=1
         )
         rows = tile_rows(span, span_length)
-        mixed[rows, :] = (gated[rows, :] + blend[rows, :] * memory).astype(jnp.bfloat16)
-
-    def merge_half(first):
-        def some(i, carry):
-            merge(first + 2 * i)
-            merge(first + 2 * i + 1)
-            return carry
-
-        lax.fori_loop(0, span_count // 4, some, 0)
-
-    merge_half((1 - core) * (span_count // 2))
-    mixed_copy = pltpu.make_async_remote_copy(
-        src_ref=mixed.at[tile_rows(1 - core, half)],
-        dst_ref=other_mixed,
-        send_sem=send_mixed,
-        recv_sem=recv_mixed,
-        device_id=(me, 1 - core),
-        device_id_type=MESH,
-    )
-    mixed_copy.start()
-    merge_half(core * (span_count // 2))
-    mine = tile_rows(core, half)
-
-    @pl.when(core == 0)
-    def _():
-        out_ref[:, :width] = mixed[mine, :]
-
-    @pl.when(core == 1)
-    def _():
-        out_ref[:, width:] = mixed[mine, :]
-
-    mixed_copy.wait()
-
-    @pl.when(core == 0)
-    def _():
-        out_ref[:, width:] = other_mixed[...]
-
-    @pl.when(core == 1)
-    def _():
-        out_ref[:, :width] = other_mixed[...]
-
+        return (gated[rows, :] + blend[rows, :] * memory).astype(jnp.bfloat16)
+
+    columns = pl.ds(pl.multiple_of(core * width, width), width)
+    half_spans = span_count // 2
+    pieces = send_mixed.shape[0]
+    per_piece = half_spans // pieces
+
+    def mixed_copy(i):
+        rows = tile_rows(i, per_piece * span_length)
+        return pltpu.make_async_remote_copy(
+            src_ref=mixed.at[rows],
+            dst_ref=out_ref.at[rows, columns],
+            send_sem=send_mixed.at[i],
+            recv_sem=recv_mixed.at[i],
+            device_id=(me, 1 - core),
+            device_id_type=MESH,
+        )
+
+    def merge_theirs(i, carry):
+        for k in range(per_piece):
+            span = i * per_piece + k
+            mixed[tile_rows(span, span_length), :] = merge((1 - core) * half_spans + span)
+
+        @pl.when(i > 0)
+        def _():
+            mixed_copy(i - 1).start()
+
+        return carry
+
+    lax.fori_loop(0, pieces, merge_theirs, 0)
+    mixed_copy(pieces - 1).start()
+
+    def merge_mine(i, carry):
+        for k in range(per_piece):
+            span = i * per_piece + k
+            out_ref[tile_rows(span, span_length), columns] = merge(core * half_spans + span)
+        return carry
+
+    lax.fori_loop(0, pieces, merge_mine, 0)
+    for i in range(pieces):
+        mixed_copy(i).wait()
     pltpu.make_async_copy(slots.at[rest], slots.at[rest], send_query).wait()
     pltpu.make_async_copy(table.at[rest], table.at[rest], send_table).wait()
     pltpu.make_async_copy(parts.at[rest], parts.at[rest], send_part).wait()
@@ -532,7 +534,7 @@
     anywhere = pl.BlockSpec(memory_space=pl.ANY)
     by_rows = pl.pallas_call(
         layer_kernel,
-        out_shape=jax.ShapeDtypeStruct((row_count // 2, 2 * width), bf16),
+        out_shape=pltpu.VMEM((row_count // 2, 2 * width), bf16),
         in_specs=[
             pl.BlockSpec(memory_space=pltpu.SMEM),
             pl.BlockSpec(memory_space=pltpu.VMEM),
@@ -575,7 +577,6 @@
             by_row,
             pltpu.VMEM((row_count, 128), f32),
             pltpu.VMEM((row_count, 128), f32),
-            pltpu.VMEM((row_count, width), bf16),
             pltpu.VMEM((row_count // 2, width), bf16),
             dma((row_count // TILE,)),
             dma((store.shape[0] // TILE,)),
@@ -583,7 +584,9 @@
             dma,
             dma((N_ST,)),
         ]
-        + [dma] * 12,
+        + [dma] * 8
+        + [dma((3,))] * 2
+        + [dma] * 2,
         compiler_params=pltpu.CompilerParams(
             collective_id=0, has_side_effects=True, vmem_limit_bytes=60 << 20
         ),

time: 74.8 us -> 69.8 us (0.933)
  Pallas kernels: 71.5 us -> 67.5 us
  matrix products: 3.12 us -> 2.13 us
    pallas_call x1, Pallas kernels: 71.5 us -> 67.5 us  [per_device(): pl.pallas_call(layer_kernel, out_shape=pltpu.VMEM((row_count // 2, 2 * wi...]
    dot_general x1, matrix products: 3.12 us -> 2.13 us  [per_device(): jnp.dot(by_rows, output_weight, preferred_element_type=f32).astype(bf16)]
where the time goes in v4:
time: 69.8 us; the launch traced here: 69.6 us
  Pallas kernels  67.5 us (97%)
  matrix products  2.13 us (3%)
    pallas_call x1, Pallas kernels, per_device(): pl.pallas_call(layer_kernel, out_shape=pltpu.VMEM((row_count // 2, 2 * wi...  67.5 us
    dot_general x1, matrix products, per_device(): jnp.dot(by_rows, output_weight, preferred_element_type=f32).astype(bf16)  2.13 us

profile of v4, /device:TPU:1, one launch (start us, length us, event | category | flops | bytes accessed | tf_op | source)
XLA Modules:
  0.0 69.6 jit_solution(5118430161946733927)
XLA Ops:
  0.0 0.0 copy-start
  0.0 67.5 %shard_map.145 = bf16[384,512]{1,0:T(8,128)(2,1)S(1)} custom-call(s32[4,12]{1,0:T(4,128)} %bitcast.12, s32[4,12]{1,0:T(4,128)} %bitcast.13, bf16[768,2048]{1,0:T(8,128)(2,1)} %tokens_hbm.1, bf16[3072,2048]{1,0:T(8,128)(2,1)} %bitcast.8, f32[1,2048]{1,0:T(1,128)} %bitcast.10, f32[1,2048]{1,0:T(1,128)} %bitcast.11, bf16[2048,256]{1,0:T(8,128)(2,1)} %carry_weight_hbm.1, ...), custom_call_target="tpu_custom_call" | custom-call | tf_op jit(solution)/shard_map/pallas_call | solution.py:535
  67.5 0.0 copy-done
  67.5 2.1 %convolution_convert_fusion = bf16[384,2048]{1,0:T(8,128)(2,1)} fusion(bf16[384,512]{1,0:T(8,128)(2,1)S(1)} %shard_map.145, bf16[512,2048]{1,0:T(8,128)(2,1)S(1)} %copy-done), kind=kOutput, calls=%fused_computation | convolution fusion | flops 806092800 | bytes 4063232 | tf_op jit(solution)/shard_map/dot_general | solution.py:610
Async XLA Ops:
  0.0 67.5 %copy-start = (bf16[512,2048]{1,0:T(8,128)(2,1)S(1)}, bf16[512,2048]{1,0:T(8,128)(2,1)}, u32[]{:S(2)}) copy-start(bf16[512,2048]{1,0:T(8,128)(2,1)} %param.29) | copy-start | bytes 6291460

commit v5 on v4

--- a/solution.py
+++ b/solution.py
@@ -14,6 +14,7 @@
 GROUP = 4
 CHUNK = 16
 TILE = 256
+AHEAD = 8
 
 
 OFFSETS = [
@@ -60,6 +61,7 @@
     key_weight_hbm,
     read_weight_hbm,
     blend_weight_hbm,
+    output_weight_hbm,
     out_ref,
     tokens,
     store,
@@ -74,6 +76,7 @@
     key_weight,
     read_weight,
     blend_weight,
+    output_weight,
     rows_normed,
     head_mask,
     queries,
@@ -97,6 +100,7 @@
     moments,
     other_moments,
     mixed,
+    by_rows,
     load_tokens,
     load_store,
     load_small,
@@ -139,11 +143,6 @@
             for j in range(GROUP)
         ]
 
-    barrier = pltpu.get_barrier_semaphore()
-    for peer in peers[1:]:
-        pl.semaphore_signal(barrier, inc=1, device_id=(peer, core), device_id_type=MESH)
-    pl.semaphore_signal(barrier, inc=1, device_id=(me, 1 - core), device_id_type=MESH)
-
     def tile_rows(i, size):
         return pl.ds(pl.multiple_of(i * size, size), size)
 
@@ -169,15 +168,22 @@
             ("blend_weight", blend_weight_hbm, blend_weight),
             ("position_mix", position_mix_hbm, position_mix),
             ("position_bias", position_bias_hbm, position_bias),
+            ("output_weight", output_weight_hbm, output_weight),
         )
     ):
         small[name] = pltpu.make_async_copy(source, target, load_small.at[n])
-    small["token_gain"].start()
     token_tiles = row_count // TILE
     store_tiles = store.shape[0] // TILE
-    for i in range(token_tiles):
+    token_load(0).start()
+    small["token_gain"].start()
+    small["query_weight"].start()
+    for i in range(1, token_tiles):
         token_load(i).start()
-    small["query_weight"].start()
+    barrier = pltpu.get_barrier_semaphore()
+    for peer in peers[1:]:
+        pl.semaphore_signal(barrier, inc=1, device_id=(peer, core), device_id_type=MESH)
+    pl.semaphore_signal(barrier, inc=1, device_id=(me, 1 - core), device_id_type=MESH)
+
 
     def start_later_loads():
         small["store_gain"].start()
@@ -192,6 +198,7 @@
             "blend_weight",
             "position_mix",
             "position_bias",
+            "output_weight",
         ):
             small[name].start()
 
@@ -230,21 +237,16 @@
 
     for i in range(token_tiles):
         token_load(i).wait()
+        if i == 1:
+            small["query_weight"].wait()
         if i == token_tiles - 1:
-            small["query_weight"].wait()
             start_later_loads()
-        norm_rows(tokens, tokens, token_gain, TILE, i * TILE, i * TILE, TILE // CHUNK if i == token_tiles - 1 else 4)
-        if i == token_tiles - 1:
-            for k in range(i):
-                token_query(k)
+        norm_rows(tokens, tokens, token_gain, TILE, i * TILE, i * TILE, TILE // CHUNK if i else 4)
+        if i:
+            token_query(i - 1)
     token_query(token_tiles - 1)
     span_copy.wait()
 
-    def fill(slot, carry):
-        slots[slot] = queries[span_smem[0, slot]]
-        return carry
-
-    lax.fori_loop(0, N_ST, fill, 0, unroll=4)
     pl.semaphore_wait(barrier, N_ST)
 
     def table_copy(peer):
@@ -269,7 +271,11 @@
 
     for peer in peers[1:]:
         table_copy(peer).start()
-    for peer in peers[1:]:
+    for k, peer in enumerate(peers):
+        if k > AHEAD:
+            query_copy(peers[k - AHEAD]).start()
+        slots[peer] = queries[span_smem[0, peer]]
+    for peer in peers[N_ST - AHEAD :]:
         query_copy(peer).start()
     asked[me] = slots[me]
 
@@ -462,7 +468,7 @@
         rows = tile_rows(i, per_piece * span_length)
         return pltpu.make_async_remote_copy(
             src_ref=mixed.at[rows],
-            dst_ref=out_ref.at[rows, columns],
+            dst_ref=by_rows.at[rows, columns],
             send_sem=send_mixed.at[i],
             recv_sem=recv_mixed.at[i],
             device_id=(me, 1 - core),
@@ -483,15 +489,28 @@
     lax.fori_loop(0, pieces, merge_theirs, 0)
     mixed_copy(pieces - 1).start()
 
+    piece_rows = per_piece * span_length
+    out_columns = 2 * TILE
+    small["output_weight"].wait()
+
     def merge_mine(i, carry):
         for k in range(per_piece):
             span = i * per_piece + k
-            out_ref[tile_rows(span, span_length), columns] = merge(core * half_spans + span)
+            by_rows[tile_rows(span, span_length), columns] = merge(core * half_spans + span)
         return carry
 
     lax.fori_loop(0, pieces, merge_mine, 0)
-    for i in range(pieces):
+
+    def finish(i, carry):
         mixed_copy(i).wait()
+        rows = tile_rows(i, piece_rows)
+        for n in range(0, out_ref.shape[1], out_columns):
+            out_ref[rows, n : n + out_columns] = jnp.dot(
+                by_rows[rows, :], output_weight[:, n : n + out_columns], preferred_element_type=jnp.float32
+            ).astype(jnp.bfloat16)
+        return carry
+
+    lax.fori_loop(0, pieces, finish, 0)
     pltpu.make_async_copy(slots.at[rest], slots.at[rest], send_query).wait()
     pltpu.make_async_copy(table.at[rest], table.at[rest], send_table).wait()
     pltpu.make_async_copy(parts.at[rest], parts.at[rest], send_part).wait()
@@ -532,14 +551,14 @@
     by_row = pltpu.VMEM((row_count, width), f32)
     dma = pltpu.SemaphoreType.DMA
     anywhere = pl.BlockSpec(memory_space=pl.ANY)
-    by_rows = pl.pallas_call(
+    return pl.pallas_call(
         layer_kernel,
-        out_shape=pltpu.VMEM((row_count // 2, 2 * width), bf16),
+        out_shape=pltpu.VMEM((row_count // 2, features), bf16),
         in_specs=[
             pl.BlockSpec(memory_space=pltpu.SMEM),
             pl.BlockSpec(memory_space=pltpu.VMEM),
         ]
-        + [anywhere] * 13,
+        + [anywhere] * 14,
         out_specs=pl.BlockSpec(memory_space=pltpu.VMEM),
         scratch_shapes=[
             pltpu.VMEM(tokens.shape, bf16),
@@ -555,6 +574,7 @@
             weight,
             weight,
             weight,
+            pltpu.VMEM(output_weight.shape, bf16),
             pltpu.VMEM((TILE, features), bf16),
             pltpu.VMEM((heads, span_length, width), bf16),
             pltpu.VMEM((span_count, span_length, width), bf16),
@@ -578,9 +598,10 @@
             pltpu.VMEM((row_count, 128), f32),
             pltpu.VMEM((row_count, 128), f32),
             pltpu.VMEM((row_count // 2, width), bf16),
+            pltpu.VMEM((row_count // 2, 2 * width), bf16),
             dma((row_count // TILE,)),
             dma((store.shape[0] // TILE,)),
-            dma((11,)),
+            dma((12,)),
             dma,
             dma((N_ST,)),
         ]
@@ -606,8 +627,8 @@
         key_weight,
         read_weight,
         blend_weight,
+        output_weight,
     )
-    return jnp.dot(by_rows, output_weight, preferred_element_type=f32).astype(bf16)
 
 
 def solution(mesh):

time: 69.8 us -> 67.7 us (0.970)
  matrix products: 2.13 us -> 0 us
  local copies, waits for them, and re-layouts: 0.01 us -> 1.15 us
  Pallas kernels: 67.5 us -> 66.5 us
    dot_general x1 -> x0, matrix products: 2.13 us -> none  [per_device(): jnp.dot(by_rows, output_weight, preferred_element_type=f32).astype(bf16)]
    unnamed x2 -> x1, local copies, waits for them, and re-layouts: 0.01 us -> 1.15 us
    pallas_call x1, Pallas kernels: 67.5 us -> 66.5 us  [per_device(): pl.pallas_call(layer_kernel, out_shape=pltpu.VMEM((row_count // 2, featur...]
where the time goes in v5:
time: 67.7 us; the launch traced here: 67.6 us
  Pallas kernels  66.5 us (98%)
  local copies, waits for them, and re-layouts  1.15 us (2%)
    pallas_call x1, Pallas kernels, per_device(): pl.pallas_call(layer_kernel, out_shape=pltpu.VMEM((row_count // 2, featur...  66.5 us

profile of v5, /device:TPU:1, one launch (start us, length us, event | category | flops | bytes accessed | tf_op | source)
XLA Modules:
  0.0 67.6 jit_solution(8415778615983008577)
XLA Ops:
  0.0 66.5 %shard_map.145 = bf16[384,2048]{1,0:T(8,128)(2,1)S(1)} custom-call(s32[4,12]{1,0:T(4,128)} %bitcast.10, s32[4,12]{1,0:T(4,128)} %bitcast.11, bf16[768,2048]{1,0:T(8,128)(2,1)} %tokens_hbm.1, bf16[3072,2048]{1,0:T(8,128)(2,1)} %bitcast.6, f32[1,2048]{1,0:T(1,128)} %bitcast.8, f32[1,2048]{1,0:T(1,128)} %bitcast.9, bf16[2048,256]{1,0:T(8,128)(2,1)} %carry_weight_hbm.1, ...), custom_call_target="tpu_custom_call" | custom-call | tf_op jit(solution)/shard_map/pallas_call | solution.py:554
  66.5 1.1 %copy.17 = bf16[384,2048]{1,0:T(8,128)(2,1)} copy(bf16[384,2048]{1,0:T(8,128)(2,1)S(1)} %shard_map.145) | data formatting | bytes 3145728

commit v6 on v5

--- a/solution.py
+++ b/solution.py
@@ -17,11 +17,12 @@
 AHEAD = 8
 
 
-OFFSETS = [
-    ((b + j) % SIDE, (a + j) % SIDE, j)
+OFFSETS = [(0, 0, 0)] + [
+    ((2 - b + 3 * j) % SIDE, (2 - a + j) % SIDE, j)
     for a in range(SIDE)
     for b in range(SIDE)
     for j in range(SIDE)
+    if (a, b, j) != (2, 2, 0)
 ]
 
 
@@ -100,7 +101,9 @@
     moments,
     other_moments,
     mixed,
-    by_rows,
+    own_mixed,
+    other_mixed,
+    own_product,
     load_tokens,
     load_store,
     load_small,
@@ -137,9 +140,9 @@
     def sources(group):
         a, b = lax.div(group, SIDE), lax.rem(group, SIDE)
         return [
-            lax.rem(my_z - b - j + 2 * SIDE, SIDE) * (SIDE * SIDE)
-            + lax.rem(my_y - a - j + 2 * SIDE, SIDE) * SIDE
-            + lax.rem(my_x - j + SIDE, SIDE)
+            lax.rem(my_z + b + j + 2, SIDE) * (SIDE * SIDE)
+            + lax.rem(my_y + a + 6 - j, SIDE) * SIDE
+            + lax.rem(my_x + SIDE - j, SIDE)
             for j in range(GROUP)
         ]
 
@@ -348,9 +351,9 @@
 
     def serve(group, carry):
         now = sources(group)
-        for j, source in enumerate(now):
-
-            @pl.when(group + j > 0)
+        for source in now:
+
+            @pl.when(source != me)
             def _(source=source):
                 pltpu.make_async_copy(asked.at[source], asked.at[source], recv_query.at[source]).wait()
 
@@ -359,17 +362,21 @@
             parts[source] = part
             logs[source] = log_total
 
-        for j, source in enumerate(sources(group - 1)):
-
-            @pl.when((group > 1) | ((group == 1) & (j > 0)))
+        @pl.when(group > 0)
+        def _():
+            send_group(group - 1)
+
+        return carry
+
+    def send_group(group):
+        for source in sources(group):
+
+            @pl.when(source != me)
             def _(source=source):
                 send_back(source)
 
-        return carry
-
     lax.fori_loop(0, N_ST // GROUP, serve, 0)
-    for source in sources(N_ST // GROUP - 1):
-        send_back(source)
+    send_group(N_ST // GROUP - 1)
     back[me] = parts[me]
     back_logs[me] = logs[me]
 
@@ -443,7 +450,7 @@
     pltpu.make_async_copy(back.at[rest], back.at[rest], recv_part).wait()
     pltpu.make_async_copy(back_logs.at[rest], back_logs.at[rest], recv_log).wait()
 
-    def merge(span):
+    def merged(span):
         owners = [lax.div(ids_smem[k, span], passage_count) for k in range(pick_count)]
         levels = [back_logs[o] for o in owners]
         top = functools.reduce(jnp.maximum, levels)
@@ -452,23 +459,37 @@
         summed = functools.reduce(
             jnp.add, [s * back[o].astype(jnp.float32) for s, o in zip(scales, owners)]
         )
-        turned = (summed / total).T
+        return summed / total
+
+    def merge(first):
+        turned = jnp.concatenate([merged(first), merged(first + 1)], axis=0).T
         memory = jnp.concatenate(
-            [turned[h * span_length : (h + 1) * span_length] for h in range(heads)], axis=1
-        )
-        rows = tile_rows(span, span_length)
+            [
+                jnp.concatenate(
+                    [
+                        turned[
+                            h * span_length : (h + 1) * span_length, s * head_dim : (s + 1) * head_dim
+                        ]
+                        for h in range(heads)
+                    ],
+                    axis=1,
+                )
+                for s in range(2)
+            ],
+            axis=0,
+        )
+        rows = pl.ds(pl.multiple_of(first * span_length, 2 * span_length), 2 * span_length)
         return (gated[rows, :] + blend[rows, :] * memory).astype(jnp.bfloat16)
 
-    columns = pl.ds(pl.multiple_of(core * width, width), width)
     half_spans = span_count // 2
-    pieces = send_mixed.shape[0]
-    per_piece = half_spans // pieces
+    pieces = half_spans // 2
+    piece_rows = 2 * span_length
 
     def mixed_copy(i):
-        rows = tile_rows(i, per_piece * span_length)
+        rows = tile_rows(i, piece_rows)
         return pltpu.make_async_remote_copy(
             src_ref=mixed.at[rows],
-            dst_ref=by_rows.at[rows, columns],
+            dst_ref=other_mixed.at[rows],
             send_sem=send_mixed.at[i],
             recv_sem=recv_mixed.at[i],
             device_id=(me, 1 - core),
@@ -476,9 +497,7 @@
         )
 
     def merge_theirs(i, carry):
-        for k in range(per_piece):
-            span = i * per_piece + k
-            mixed[tile_rows(span, span_length), :] = merge((1 - core) * half_spans + span)
+        mixed[tile_rows(i, piece_rows), :] = merge((1 - core) * half_spans + 2 * i)
 
         @pl.when(i > 0)
         def _():
@@ -489,28 +508,28 @@
     lax.fori_loop(0, pieces, merge_theirs, 0)
     mixed_copy(pieces - 1).start()
 
-    piece_rows = per_piece * span_length
-    out_columns = 2 * TILE
     small["output_weight"].wait()
 
     def merge_mine(i, carry):
-        for k in range(per_piece):
-            span = i * per_piece + k
-            by_rows[tile_rows(span, span_length), columns] = merge(core * half_spans + span)
+        own_mixed[tile_rows(i, piece_rows), :] = merge(core * half_spans + 2 * i)
         return carry
 
     lax.fori_loop(0, pieces, merge_mine, 0)
 
-    def finish(i, carry):
+    def product(rows, which, part):
+        return jnp.dot(
+            rows[...], output_weight[tile_rows(which, width), part], preferred_element_type=jnp.float32
+        )
+
+    parts_of_out = [slice(0, out_ref.shape[1])]
+    for part in parts_of_out:
+        own_product[:, part] = product(own_mixed, core, part)
+    for i in range(pieces):
         mixed_copy(i).wait()
-        rows = tile_rows(i, piece_rows)
-        for n in range(0, out_ref.shape[1], out_columns):
-            out_ref[rows, n : n + out_columns] = jnp.dot(
-                by_rows[rows, :], output_weight[:, n : n + out_columns], preferred_element_type=jnp.float32
-            ).astype(jnp.bfloat16)
-        return carry
-
-    lax.fori_loop(0, pieces, finish, 0)
+    for part in parts_of_out:
+        out_ref[:, part] = (own_product[:, part] + product(other_mixed, 1 - core, part)).astype(
+            jnp.bfloat16
+        )
     pltpu.make_async_copy(slots.at[rest], slots.at[rest], send_query).wait()
     pltpu.make_async_copy(table.at[rest], table.at[rest], send_table).wait()
     pltpu.make_async_copy(parts.at[rest], parts.at[rest], send_part).wait()
@@ -598,7 +617,9 @@
             pltpu.VMEM((row_count, 128), f32),
             pltpu.VMEM((row_count, 128), f32),
             pltpu.VMEM((row_count // 2, width), bf16),
-            pltpu.VMEM((row_count // 2, 2 * width), bf16),
+            pltpu.VMEM((row_count // 2, width), bf16),
+            pltpu.VMEM((row_count // 2, width), bf16),
+            pltpu.VMEM((row_count // 2, features), f32),
             dma((row_count // TILE,)),
             dma((store.shape[0] // TILE,)),
             dma((12,)),

time: 67.7 us -> 67.3 us (level)
  no operation moved by 1% of the time
where the time goes in v6:
time: 67.3 us; the launch traced here: 67.2 us
  Pallas kernels  66 us (98%)
  local copies, waits for them, and re-layouts  1.15 us (2%)
    pallas_call x1, Pallas kernels, per_device(): pl.pallas_call(layer_kernel, out_shape=pltpu.VMEM((row_count // 2, featur...  66 us

profile of v6, /device:TPU:1, one launch (start us, length us, event | category | flops | bytes accessed | tf_op | source)
XLA Modules:
  0.0 67.2 jit_solution(2428195044130257458)
XLA Ops:
  0.0 66.0 %shard_map.145 = bf16[384,2048]{1,0:T(8,128)(2,1)S(1)} custom-call(s32[4,12]{1,0:T(4,128)} %bitcast.10, s32[4,12]{1,0:T(4,128)} %bitcast.11, bf16[768,2048]{1,0:T(8,128)(2,1)} %tokens_hbm.1, bf16[3072,2048]{1,0:T(8,128)(2,1)} %bitcast.6, f32[1,2048]{1,0:T(1,128)} %bitcast.8, f32[1,2048]{1,0:T(1,128)} %bitcast.9, bf16[2048,256]{1,0:T(8,128)(2,1)} %carry_weight_hbm.1, ...), custom_call_target="tpu_custom_call" | custom-call | tf_op jit(solution)/shard_map/pallas_call | solution.py:573
  66.0 1.1 %copy.17 = bf16[384,2048]{1,0:T(8,128)(2,1)} copy(bf16[384,2048]{1,0:T(8,128)(2,1)S(1)} %shard_map.145) | data formatting | bytes 3145728
